TPU v7x, 256 devices: a whole 4x4x8 slice. The times are simulated.
256 devices in a mesh: sp: 16 (over y, x), tp: 16 (over z, core).
Axes of the slice: x: 4, y: 4, z: 8, core: 2. Of those that a mesh axis runs over, the one named last changes fastest.
Arguments:
- out_gate: bfloat16 [8192, 2048], P('sp', 'tp'), may hold values from -6 to 6
- in_gate: bfloat16 [8192, 2048], P('sp', 'tp'), may hold values from -6 to 6
- conv_input: bfloat16 [8192, 2048], P('sp', 'tp'), may hold values from -6 to 6
- conv_taps: bfloat16 [3, 2048], P(None, 'tp'), may hold values from -3.5 to 3.5
- documents: int32 [8192], P('sp'), may hold values from 0 to 8, never falling along the last dimension, each value on 1 to 1536 neighbouring positions
- out_weight: bfloat16 [2048, 2048], P('tp'), may hold values from -0.125 to 0.125
- residual: bfloat16 [8192, 2048], P(('sp', 'tp')), may hold values from -6 to 6
- norm_gain: bfloat16 [2048], replicated, may hold values from 0.099609375 to 1.8984375
- expert_ids: int32 [8192, 2], P(('sp', 'tp')), may hold values from 0 to 15, all different within a row; in each aligned block of 32 rows (0 to 31, 32 to 63, ...) at most 6 rows name the same one
- route_weights: float32 [8192, 2], P(('sp', 'tp')), may hold values from 0.1 to 1
- gate_weight: bfloat16 [16, 2048, 4096], P('sp', None, 'tp'), may hold values from -0.125 to 0.125
- up_weight: bfloat16 [16, 2048, 4096], P('sp', None, 'tp'), may hold values from -0.125 to 0.125
- down_weight: bfloat16 [16, 4096, 2048], P('sp', 'tp'), may hold values from -0.09375 to 0.09375
Outputs:
- layer_out: bfloat16 [8192, 2048], P(('sp', 'tp'))
Inputs may be any that keep to these rules, and one draw needn't show every extreme that they name: `expert_ids`: A token's two experts differ; in each aligned block of 32 rows no expert is named by more than 6 entries, a bound that some block reaches. `documents`: document numbers never fall along the sequence; a document holds at most 1536 positions.
All inputs are finite; a program needn't handle non-finite values.
Results may differ from a plain program's by a relative error of at most 0.017.
Values may be sent and summed in bfloat16 or wider, within the bound.
A program may use at most 64 MiB of HBM per device.

v0:
```python
import jax
import jax.numpy as jnp
from jax import lax
from jax.sharding import PartitionSpec as P

EPS = 1e-06


def passed_along(block, axis, distance):
    devices = range(lax.axis_size(axis))
    route = [(i - distance, i) for i in devices if i - distance in devices]
    return lax.ppermute(block, axis, route)


def split_up(x, dim, count):
    before, after = (x.shape[:dim], x.shape[dim + 1 :])
    return jnp.moveaxis(x.reshape(*before, count, -1, *after), dim, 0)


def summed_on_arrival(x, axis, dim):
    count = lax.axis_size(axis)
    parts = lax.all_to_all(split_up(x, dim, count), axis, 0, 0, tiled=True)
    return jnp.sum(parts.astype(jnp.float32), axis=0)


def slot_index(expert_ids, experts, capacity):
    listed = expert_ids.reshape(-1)
    onehot = (listed[:, None] == jnp.arange(experts, dtype=jnp.int32)[None, :]).astype(jnp.int32)
    earlier = jnp.cumsum(onehot, axis=0) - onehot
    within = jnp.sum(earlier * onehot, axis=1)
    return listed * capacity + within


def shards(
    out_gate,
    in_gate,
    conv_input,
    conv_taps,
    documents,
    out_weight,
    residual,
    norm_gain,
    expert_ids,
    route_weights,
    gate_weight,
    up_weight,
    down_weight,
):
    length = conv_input.shape[0]
    signal = in_gate.astype(jnp.float32) * conv_input.astype(jnp.float32)
    doc_values = documents.astype(jnp.float32)
    prior_signal, prior_docs = passed_along(
        (signal[length - 2 :], doc_values[length - 2 :]), "sp", 1
    )
    long_signal = jnp.concatenate([prior_signal, signal], axis=0)
    long_docs = jnp.concatenate([prior_docs, doc_values], axis=0)
    position = lax.axis_index("sp") * length + jnp.arange(length, dtype=jnp.int32)
    tap_values = conv_taps.astype(jnp.float32)
    mixed_conv = tap_values[2][None, :] * signal
    for offset in (1, 2):
        earlier_signal = long_signal[2 - offset : 2 - offset + length]
        earlier_docs = long_docs[2 - offset : 2 - offset + length]
        allowed = (position >= offset) & (earlier_docs == doc_values)
        mixed_conv = mixed_conv + jnp.where(
            allowed[:, None], tap_values[2 - offset][None, :] * earlier_signal, 0.0
        )
    gated = (out_gate.astype(jnp.float32) * mixed_conv).astype(jnp.bfloat16)
    block_rows = length // lax.axis_size("tp")
    mixed = summed_on_arrival(
        jnp.dot(gated, out_weight, preferred_element_type=jnp.float32).astype(jnp.bfloat16), "tp", 0
    )
    hidden_wide = (residual.astype(jnp.float32) + mixed).astype(jnp.bfloat16).astype(jnp.float32)
    stats = jnp.mean(hidden_wide * hidden_wide, axis=-1, keepdims=True)
    normed = (hidden_wide * lax.rsqrt(stats + EPS) * norm_gain.astype(jnp.float32)[None, :]).astype(
        jnp.bfloat16
    )
    model_width = normed.shape[1]
    experts = lax.axis_size("sp")
    capacity = max(2, (3 * block_rows + experts - 1) // experts)
    target = slot_index(expert_ids, experts, capacity)
    slots = jnp.arange(experts * capacity, dtype=jnp.int32)
    table = jnp.sum(
        (target.reshape(block_rows, 2)[:, :, None] == slots[None, None, :]).astype(jnp.bfloat16),
        axis=1,
    )
    outgoing = lax.dot_general(
        table, normed, (((0,), (0,)), ((), ())), preferred_element_type=jnp.float32
    ).astype(jnp.bfloat16)
    arrived = lax.all_to_all(outgoing, "sp", split_axis=0, concat_axis=0, tiled=True)
    gathered = lax.all_gather(arrived, "tp", axis=0, tiled=True)
    gate_proj = jnp.dot(gathered, gate_weight[0], preferred_element_type=jnp.float32)
    up_proj = jnp.dot(gathered, up_weight[0], preferred_element_type=jnp.float32)
    act = (jax.nn.silu(gate_proj) * up_proj).astype(jnp.bfloat16)
    summed = lax.psum_scatter(
        jnp.dot(act, down_weight[0], preferred_element_type=jnp.float32).astype(jnp.bfloat16),
        "tp",
        scatter_dimension=0,
        tiled=True,
    )
    returned = lax.all_to_all(summed, "sp", split_axis=0, concat_axis=0, tiled=True)
    picked = returned[target].astype(jnp.float32).reshape(block_rows, 2, model_width)
    combined = jnp.sum(picked * route_weights[:, :, None], axis=1)
    return (hidden_wide + combined).astype(jnp.bfloat16)


def solution(mesh):
    in_specs = (
        P("sp", "tp"),
        P("sp", "tp"),
        P("sp", "tp"),
        P(None, "tp"),
        P("sp"),
        P("tp", None),
        P(("sp", "tp"), None),
        P(),
        P(("sp", "tp"), None),
        P(("sp", "tp"), None),
        P("sp", None, "tp"),
        P("sp", None, "tp"),
        P("sp", "tp", None),
    )
    out_specs = P(("sp", "tp"), None)
    return jax.shard_map(shards, mesh=mesh, in_specs=in_specs, out_specs=out_specs, check_vma=False)
```

profile of v0, /device:TPU:2, one launch (start us, length us, event | category | flops | bytes accessed | tf_op | source)
XLA Modules:
  0.0 251.5 jit_solution(9978602390221171787)
XLA Ops:
  6.5 0.8 convert_element_type.71
  7.3 0.1 slice.28
  7.4 3.4 %collective-permute-start = (f32[2]{0:T(128)S(1)}, f32[2]{0:T(128)S(1)}, u32[]{:S(2)}, u32[]{:S(2)}) collective-permute-start(f32[2]{0:T(128)S(1)} %slice.28), channel_id=1, source_target_pairs={{0,16},{16,32},{32,48},{48,64},{64,80},{80,96},{96,112},{112,128},... | collective-permute-start | bytes 32 | tf_op jit(solution)/shard_map/ppermute | solution.py:12
  10.8 1.0 convert_multiply_fusion.2
  11.8 3.1 %collective-permute-start.1 = (f32[2,128]{1,0:T(2,128)S(1)}, f32[2,128]{1,0:T(2,128)S(1)}, u32[]{:S(2)}, u32[]{:S(2)}) collective-permute-start(f32[2,128]{1,0:T(2,128)S(1)} %slice.38), channel_id=1, source_target_pairs={{0,16},{16,32},{32,48},{48,64},{64,80},{80,96},{96,112},{112,128},... | collective-permute-start | bytes 3080 | tf_op jit(solution)/shard_map/ppermute | solution.py:12
  14.9 0.7 convert_element_type.68
  15.6 0.0 collective-permute-done
  15.6 0.1 pad_maximum_fusion.1
  15.7 0.8 fusion.35
  16.4 0.8 collective-permute-done.1
  17.3 3.2 %convolution_convert_fusion.1 = bf16[512,2048]{1,0:T(8,128)(2,1)} fusion(bf16[128,2048]{1,0:T(8,128)(2,1)} %param.18, f32[2,128]{1,0:T(2,128)S(1)} %collective-permute-done.1, f32[512,128]{1,0:T(8,128)S(1)} %convert_multiply_fusion.2, bf16[512,128]{1,0:T(8,128)(2,1)} %param.13, f32[128]{0:T(128)S(1)} %get-tuple-element.12, f32[128]{0:T(128)S(1)} %get-tuple-element.13, ...), kind=kOutput, calls=%fused_computation.3 | convolution fusion | flops 270270464 | bytes 3018240 | tf_op jit(solution)/shard_map/dot_general | solution.py:70
  20.5 8.7 %all-to-all-start = ((bf16[16,32,2048]{2,1,0:T(8,128)(2,1)}), bf16[16,32,2048]{2,1,0:T(8,128)(2,1)S(1)}, u32[]{:S(2)}, u32[]{:S(2)}) async-start(bf16[16,32,2048]{2,1,0:T(8,128)(2,1)} %bitcast.3), calls=%async_computation | async-start | bytes 4194304 | tf_op jit(solution)/shard_map/all_to_all | solution.py:22
  29.2 0.0 copy-start.1
  29.2 0.0 all-gather.2.cloned.1.call-start
  29.3 0.1 copy.20
  29.3 0.1 eq.36
  29.5 0.1 fusion.30
  29.5 0.1 reduce_window_sum.11
  29.6 0.2 select_reduce_fusion
  29.8 0.1 reduce_sum.54
  29.9 0.1 copy.22
  30.0 0.1 fusion.32
  30.1 48.3 %all-to-all-done = bf16[16,32,2048]{2,1,0:T(8,128)(2,1)S(1)} async-done(((bf16[16,32,2048]{2,1,0:T(8,128)(2,1)}), bf16[16,32,2048]{2,1,0:T(8,128)(2,1)S(1)}, u32[]{:S(2)}, u32[]{:S(2)}) %all-to-all-start) | async-done | bytes 2097184 | tf_op jit(solution)/shard_map/all_to_all | solution.py:22
  78.4 0.4 convert_reduce_fusion
  78.8 0.0 copy-start.5
  78.8 0.2 fusion.14
  79.0 0.3 convolution_convert_fusion.2
  79.3 0.1 all_to_all.20
  79.5 17.5 %all_to_all.29 = bf16[16,6,2048]{2,1,0:T(8,128)(2,1)S(1)} all-to-all(bf16[16,6,2048]{2,1,0:T(8,128)(2,1)S(1)} %all_to_all.20), channel_id=1, replica_groups=mesh['sp'=16,'tp'=16] {'sp'}, dimensions={0} | all-to-all | bytes 786432 | tf_op jit(solution)/shard_map/all_to_all | solution.py:89
  97.0 0.9 all_to_all.22
  97.9 0.0 all-gather.2.cloned.1.call-update
  97.9 0.0 copy-start.6
  97.9 0.0 reduce-scatter.2.cloned.1.call-start
  98.0 42.1 %all-gather.2.cloned.1.call-done = bf16[1536,2048]{1,0:T(8,128)(2,1)} async-done(((bf16[96,2048]{1,0:T(8,128)(2,1)}), bf16[1536,2048]{1,0:T(8,128)(2,1)}) %all-gather.2.cloned.1.call-update) | async-done | bytes 6291472 | tf_op jit(solution)/shard_map/all_gather | solution.py:90
  140.1 5.8 %fusion.4 = f32[1536,256]{1,0:T(8,128)} fusion(bf16[1536,2048]{1,0:T(8,128)(2,1)} %all-gather.2.cloned.1.call-done, bf16[1,2048,256]{2,1,0:T(8,128)(2,1)S(1)} %copy-done.5), kind=kOutput, calls=%fused_computation.9 | convolution fusion | flops 1610612736 | bytes 8912896 | tf_op jit(solution)/shard_map/dot_general | solution.py:91
  145.9 12.3 %convolution_convert_fusion = bf16[1536,2048]{1,0:T(8,128)(2,1)} fusion(bf16[1536,2048]{1,0:T(8,128)(2,1)} %all-gather.2.cloned.1.call-done, f32[1536,256]{1,0:T(8,128)} %fusion.4, bf16[1,256,2048]{2,1,0:T(8,128)(2,1)S(1)} %copy-done, bf16[1,2048,256]{2,1,0:T(8,128)(2,1)S(1)} %copy-done.6), kind=kOutput, calls=%fused_computation.1 | convolution fusion | flops 3226730496 | bytes 16252928 | tf_op jit(solution)/shard_map/dot_general | solution.py:95
  158.2 0.0 reduce-scatter.2.cloned.1.call-update
  158.2 65.9 %reduce-scatter.2.cloned.1.call-done = bf16[96,2048]{1,0:T(8,128)(2,1)} async-done(((bf16[1536,2048]{1,0:T(8,128)(2,1)}), bf16[96,2048]{1,0:T(8,128)(2,1)}) %reduce-scatter.2.cloned.1.call-update) | async-done | bytes 393232 | tf_op jit(solution)/shard_map/reduce_scatter | solution.py:94
  224.0 1.9 all_to_all.23
  226.0 7.3 %all-to-all-start.2 = ((bf16[16,6,2048]{2,1,0:T(8,128)(2,1)}), bf16[16,6,2048]{2,1,0:T(8,128)(2,1)S(1)}, u32[]{:S(2)}, u32[]{:S(2)}) async-start(bf16[16,6,2048]{2,1,0:T(8,128)(2,1)} %all_to_all.23), calls=%async_computation.3 | async-start | bytes 1048576 | tf_op jit(solution)/shard_map/all_to_all | solution.py:100
  233.2 0.1 mul.116
  233.4 0.1 copy.23
  233.5 8.6 %all-to-all-done.2 = bf16[16,6,2048]{2,1,0:T(8,128)(2,1)S(1)} async-done(((bf16[16,6,2048]{2,1,0:T(8,128)(2,1)}), bf16[16,6,2048]{2,1,0:T(8,128)(2,1)S(1)}, u32[]{:S(2)}, u32[]{:S(2)}) %all-to-all-start.2) | async-done | bytes 393248 | tf_op jit(solution)/shard_map/all_to_all | solution.py:100
  242.0 0.1 all_to_all.25
  242.2 0.7 gather_fusion
  242.9 0.3 reshape.60
  243.3 0.7 multiply_reduce_fusion
  244.0 0.7 fusion.17
  (18 shorter events, 0.1 us)
Async XLA Ops:
  6.5 139.3 %copy-start = (bf16[1,256,2048]{2,1,0:T(8,128)(2,1)S(1)}, bf16[1,256,2048]{2,1,0:T(8,128)(2,1)}, u32[]{:S(2)}) copy-start(bf16[1,256,2048]{2,1,0:T(8,128)(2,1)} %param.25) | copy-start | bytes 3145732
  7.4 8.2 %collective-permute-start = (f32[2]{0:T(128)S(1)}, f32[2]{0:T(128)S(1)}, u32[]{:S(2)}, u32[]{:S(2)}) collective-permute-start(f32[2]{0:T(128)S(1)} %slice.28), channel_id=1, source_target_pairs={{0,16},{16,32},{32,48},{48,64},{64,80},{80,96},{96,112},{112,128},... | collective-permute-start | bytes 32 | tf_op jit(solution)/shard_map/ppermute | solution.py:12
  11.8 5.5 %collective-permute-start.1 = (f32[2,128]{1,0:T(2,128)S(1)}, f32[2,128]{1,0:T(2,128)S(1)}, u32[]{:S(2)}, u32[]{:S(2)}) collective-permute-start(f32[2,128]{1,0:T(2,128)S(1)} %slice.38), channel_id=1, source_target_pairs={{0,16},{16,32},{32,48},{48,64},{64,80},{80,96},{96,112},{112,128},... | collective-permute-start | bytes 3080 | tf_op jit(solution)/shard_map/ppermute | solution.py:12
  20.5 8.8 %copy-start.3 = (s32[32,2]{0,1:T(2,128)S(1)}, s32[32,2]{0,1:T(2,128)}, u32[]{:S(2)}) copy-start(s32[32,2]{0,1:T(2,128)} %param.21) | copy-start | bytes 772
  20.5 9.5 %copy-start.2 = (bf16[2048]{0:T(1024)(128)(2,1)S(1)}, bf16[2048]{0:T(1024)(128)(2,1)}, u32[]{:S(2)}) copy-start(bf16[2048]{0:T(1024)(128)(2,1)} %param.20) | copy-start | bytes 12292
  20.5 57.9 %all-to-all-start = ((bf16[16,32,2048]{2,1,0:T(8,128)(2,1)}), bf16[16,32,2048]{2,1,0:T(8,128)(2,1)S(1)}, u32[]{:S(2)}, u32[]{:S(2)}) async-start(bf16[16,32,2048]{2,1,0:T(8,128)(2,1)} %bitcast.3), calls=%async_computation | async-start | bytes 4194304 | tf_op jit(solution)/shard_map/all_to_all | solution.py:22
  29.2 49.6 %copy-start.1 = (bf16[32,2048]{1,0:T(8,128)(2,1)S(1)}, bf16[32,2048]{1,0:T(8,128)(2,1)}, u32[]{:S(2)}) copy-start(bf16[32,2048]{1,0:T(8,128)(2,1)} %param.19) | copy-start | bytes 393220
  29.2 110.9 %all-gather.2.cloned.1.call-start = ((), (), s32[]{:S(2)}) async-start(), calls=%async_computation.4 | async-start | bytes 6684672 | tf_op jit(solution)/shard_map/all_gather | solution.py:90
  78.8 61.2 %copy-start.5 = (bf16[1,2048,256]{2,1,0:T(8,128)(2,1)S(1)}, bf16[1,2048,256]{2,1,0:T(8,128)(2,1)}, u32[]{:S(2)}) copy-start(bf16[1,2048,256]{2,1,0:T(8,128)(2,1)} %param.23) | copy-start | bytes 3145732
  97.9 48.0 %copy-start.6 = (bf16[1,2048,256]{2,1,0:T(8,128)(2,1)S(1)}, bf16[1,2048,256]{2,1,0:T(8,128)(2,1)}, u32[]{:S(2)}) copy-start(bf16[1,2048,256]{2,1,0:T(8,128)(2,1)} %param.24) | copy-start | bytes 3145732
  97.9 126.1 %reduce-scatter.2.cloned.1.call-start = ((), (), s32[]{:S(2)}) async-start(), calls=%async_computation.5 | async-start | bytes 6684672 | tf_op jit(solution)/shard_map/reduce_scatter | solution.py:94
  158.2 75.2 %copy-start.4 = (f32[32,2]{0,1:T(2,128)S(1)}, f32[32,2]{0,1:T(2,128)}, u32[]{:S(2)}) copy-start(f32[32,2]{0,1:T(2,128)} %param.22) | copy-start | bytes 772
  226.0 16.1 %all-to-all-start.2 = ((bf16[16,6,2048]{2,1,0:T(8,128)(2,1)}), bf16[16,6,2048]{2,1,0:T(8,128)(2,1)S(1)}, u32[]{:S(2)}, u32[]{:S(2)}) async-start(bf16[16,6,2048]{2,1,0:T(8,128)(2,1)} %all_to_all.23), calls=%async_computation.3 | async-start | bytes 1048576 | tf_op jit(solution)/shard_map/all_to_all | solution.py:100
Sparse Core Ops, SparseCore 0:
  98.0 41.9 all-gather.1
  158.3 65.6 reduce-scatter.1
where the time goes:
time: 252 us
  waiting for transfers between devices  166 us (66%)
  starting transfers between devices  22.6 us (9%)
  matrix products  21.6 us (9%)
  blocking collectives  17.5 us (7%)
  between operations  13.6 us (5%)
  other arithmetic  5.69 us (2%)
  local copies, waits for them, and re-layouts  4.83 us (2%)
    reduce_scatter x1, waiting for transfers between devices, shards(): lax.psum_scatter(jnp.dot(act, down_weight[0], preferred_element_type=jnp....  65.9 us
    all_to_all x1, waiting for transfers between devices, summed_on_arrival(): parts = lax.all_to_all(split_up(x, dim, count), axis, 0, 0, tiled=True)  48.3 us
    all_gather x1, waiting for transfers between devices, shards(): gathered = lax.all_gather(arrived, 'tp', axis=0, tiled=True)  42.1 us
    all_to_all x1, blocking collectives, shards(): lax.all_to_all(outgoing, 'sp', split_axis=0, concat_axis=0, tiled=True)  17.5 us
    dot_general x1, matrix products, shards(): jnp.dot(act, down_weight[0], preferred_element_type=jnp.float32)  12.3 us
    all_to_all x1, starting transfers between devices, summed_on_arrival(): parts = lax.all_to_all(split_up(x, dim, count), axis, 0, 0, tiled=True)  8.7 us
    all_to_all x1, waiting for transfers between devices, shards(): lax.all_to_all(summed, 'sp', split_axis=0, concat_axis=0, tiled=True)  8.56 us
    all_to_all x1, starting transfers between devices, shards(): lax.all_to_all(summed, 'sp', split_axis=0, concat_axis=0, tiled=True)  7.28 us
  transfers between devices with their start and end apart: 6, of which 5 were waited for; matrix products, arithmetic and copies ran while one was open for 1% of the time, Pallas kernels for 0%

commit v1 on v0

v1 whole, which is shorter than its diff:
```python
import jax
import jax.numpy as jnp
from jax import lax
from jax.experimental import pallas as pl
from jax.experimental.pallas import tpu as pltpu
from jax.sharding import PartitionSpec as P

EPS = 1e-06
MESH = pl.DeviceIdType.MESH
F32 = jnp.float32
BF16 = jnp.bfloat16

GATHER = {0: ((0, 1, 2, 3), (0, 7, 6)), 1: ((0, 1, 2), (0, 7, 6, 5))}
REDUCE = {0: ((4, 5, 6, 7), (3, 2, 1)), 1: ((5, 6, 7), (4, 3, 2, 1))}


def dot(a, b):
    return jnp.dot(a, b, preferred_element_type=F32)


def dot_t(a, b):
    return lax.dot_general(a, b, (((0,), (0,)), ((), ())), preferred_element_type=F32)


def kernel(
    og_ref, ig_ref, ci_ref, taps_ref, docs_ref, ow_ref, res_ref, gain_ref, ids_ref, rw_ref, gw_ref, uw_ref, dw_ref,
    out_ref,
    h_ig, h_ci, h_docs, ext, extd, gbuf, xa, wa, part1, rbuf1, hid, nrm,
    tmain, ttail, sel, outg, xbuf, x2, act, wg, wu, wd, part, rbuf, ret,
    loc_sem, halo_s, halo_r, duo_s, duo_r, rs1_s, rs1_r, disp_s, disp_r, ag_s, ag_r, rs_s, rs_r, ret_s, ret_r,
):
    sp = lax.axis_index("sp")
    tp = lax.axis_index("tp")
    n_sp = lax.axis_size("sp")
    core = lax.rem(tp, 2)
    z = tp // 2
    right = {"tp": lax.rem(z + 1, 8) * 2 + core}
    left = {"tp": lax.rem(z + 7, 8) * 2 + core}
    partner = {"tp": z * 2 + 1 - core}

    def sp_at(d):
        return {"sp": lax.rem(sp + d, n_sp)}

    def remote(src, dst, ssem, rsem, device):
        return pltpu.make_async_remote_copy(
            src_ref=src, dst_ref=dst, send_sem=ssem, recv_sem=rsem, device_id=device, device_id_type=MESH
        )

    local = [
        pltpu.make_async_copy(ow_ref, wa.at[0], loc_sem.at[0]),
        pltpu.make_async_copy(gw_ref.at[0], wg.at[0], loc_sem.at[1]),
        pltpu.make_async_copy(uw_ref.at[0], wu.at[0], loc_sem.at[2]),
        pltpu.make_async_copy(dw_ref.at[0], wd.at[0], loc_sem.at[3]),
    ]
    for c in local:
        c.start()

    barrier = pltpu.get_barrier_semaphore()
    for device in [right, left, partner]:
        pl.semaphore_signal(barrier, inc=1, device_id=device, device_id_type=MESH)
    for d in range(1, 16):
        pl.semaphore_signal(barrier, inc=1, device_id=sp_at(d), device_id_type=MESH)
    pl.semaphore_wait(barrier, 18)

    halo = [
        remote(ig_ref.at[pl.ds(496, 16)], h_ig, halo_s.at[0], halo_r.at[0], sp_at(1)),
        remote(ci_ref.at[pl.ds(496, 16)], h_ci, halo_s.at[1], halo_r.at[1], sp_at(1)),
        remote(docs_ref, h_docs, halo_s.at[2], halo_r.at[2], sp_at(1)),
    ]
    for c in halo:
        c.start()
    w_duo = remote(ow_ref, wa.at[1], duo_s.at[0], duo_r.at[0], partner)
    w_duo.start()

    rows = lax.broadcasted_iota(jnp.int32, (128, 32), 0)
    rel, sub = rows // 8, lax.rem(rows, 8)
    rid = lax.rem(ids_ref[...] - sp + 16, 16)
    one = [(jnp.broadcast_to(rid[k : k + 1, :], (128, 32)) == rel) for k in range(2)]
    both = (one[0] | one[1]).astype(F32)
    before = (
        lax.broadcasted_iota(jnp.int32, (32, 32), 0) < lax.broadcasted_iota(jnp.int32, (32, 32), 1)
    ).astype(BF16)
    place = dot(both.astype(BF16), before)
    hit = [jnp.where(place == sub.astype(F32), 1.0, 0.0)]
    for j in range(3):
        hit.append(
            jnp.where(((sub == 6) & (place == float(j))) | ((sub == 7) & (place == j + 3.0)), 1.0, 0.0)
        )
    hit[0] = jnp.where(sub < 6, hit[0], 0.0)
    tmain[...] = (hit[0] * both).astype(BF16)
    for j in range(3):
        ttail[j] = (hit[1 + j] * both).astype(BF16)
    sr = lax.broadcasted_iota(jnp.int32, (128, 128), 0)
    sc = lax.broadcasted_iota(jnp.int32, (128, 128), 1)
    same = (sr // 8) == (sc // 8)
    rr, rc = lax.rem(sr, 8), lax.rem(sc, 8)
    for j in range(3):
        sel[j] = jnp.where(
            same & (((rr == j) & (rc == 6)) | ((rr == j + 3) & (rc == 7))), 1.0, 0.0
        ).astype(BF16)
        sel[3 + j] = jnp.where(
            same & (((rc == j) & (rr == 6)) | ((rc == j + 3) & (rr == 7))), 1.0, 0.0
        ).astype(BF16)

    sig = ig_ref[...].astype(F32) * ci_ref[...].astype(F32)
    ext[pl.ds(16, 512), :] = sig
    docs = docs_ref[...].astype(F32)
    for i in range(4):
        extd[pl.ds(16 + 128 * i, 128), :] = jnp.broadcast_to(docs[i : i + 1, :], (128, 128)).T
    for c in halo:
        c.wait_recv()
    ext[pl.ds(0, 16), :] = h_ig[...].astype(F32) * h_ci[...].astype(F32)
    old = jnp.broadcast_to(h_docs[...].astype(F32)[3:4, :], (128, 128)).T
    extd[pl.ds(0, 16), :] = old[112:128, :]
    taps = taps_ref[...].astype(F32)
    pos = sp * 512 + lax.broadcasted_iota(jnp.int32, (512, 128), 0)
    now = extd[pl.ds(16, 512), :]
    conv = taps[2:3, :] * sig
    for off in (1, 2):
        ok = (pos >= off) & (extd[pl.ds(16 - off, 512), :] == now)
        conv = conv + jnp.where(ok, taps[2 - off : 3 - off, :] * ext[pl.ds(16 - off, 512), :], 0.0)
    gated = (og_ref[...].astype(F32) * conv).astype(BF16)
    for j in range(16):
        gbuf[j % 2, pl.ds(32 * (j // 2), 32), :] = gated[32 * j : 32 * j + 32, :]
    g_duo = remote(gbuf.at[1 - core], gbuf.at[2], duo_s.at[1], duo_r.at[1], partner)
    g_duo.start()
    xa[:, pl.ds(0, 128)] = gbuf[core]

    local[0].wait()
    w_duo.wait_recv()
    g_duo.wait_recv()
    xa[:, pl.ds(128, 128)] = gbuf[2]
    for p in range(4):
        cols = pl.ds(512 * p, 512)
        prod = dot(xa[:, pl.ds(0, 128)], wa[0, :, cols]) + dot(xa[:, pl.ds(128, 128)], wa[1, :, cols])
        part1[p] = prod.astype(BF16).reshape(8, 32, 512)
    e_duo = [
        remote(gw_ref.at[0], wg.at[1], duo_s.at[2], duo_r.at[2], partner),
        remote(uw_ref.at[0], wu.at[1], duo_s.at[3], duo_r.at[3], partner),
        remote(dw_ref.at[0], wd.at[1], duo_s.at[4], duo_r.at[4], partner),
    ]
    for c in e_duo:
        c.start()

    pending = [w_duo, g_duo] + halo + e_duo

    def reduce_hop(piece, way, hop, part_at, rbuf_at, ssem, rsem):
        slots = REDUCE[piece % 2][way]
        here = part_at(piece, slots[hop])
        if hop > 0:
            c = remote(here, rbuf_at(piece, way, hop - 1), ssem.at[piece, way, hop - 1], rsem.at[piece, way, hop - 1],
                       (right, left)[way])
            c.wait_recv()
            here[...] = (here[...].astype(F32) + rbuf_at(piece, way, hop - 1)[...].astype(F32)).astype(BF16)
        c = remote(here, rbuf_at(piece, way, hop), ssem.at[piece, way, hop], rsem.at[piece, way, hop],
                   (right, left)[way])
        c.start()
        pending.append(c)

    def reduce_tick(t, pieces, *rest):
        for piece in pieces:
            for way in range(2):
                hop = t - (4 - len(REDUCE[piece % 2][way]))
                if hop >= 0:
                    reduce_hop(piece, way, hop, *rest)

    def reduce_last(piece, part_at, rbuf_at, ssem, rsem):
        total = part_at(piece, 0)[...].astype(F32)
        for way in range(2):
            hop = len(REDUCE[piece % 2][way]) - 1
            here = rbuf_at(piece, way, hop)
            remote(here, here, ssem.at[piece, way, hop], rsem.at[piece, way, hop], (right, left)[way]).wait_recv()
            total = total + here[...].astype(F32)
        return total

    args1 = (
        lambda p, s: part1.at[p, lax.rem(z - s + 8, 8)],
        lambda p, w, h: rbuf1.at[p, w, h],
        rs1_s,
        rs1_r,
    )
    for t in range(4):
        reduce_tick(t, range(4), *args1)
    square = jnp.zeros((32, 1), F32)
    for p in range(4):
        cols = pl.ds(512 * p, 512)
        wide = (res_ref[:, cols].astype(F32) + reduce_last(p, *args1)).astype(BF16)
        hid[:, cols] = wide
        wide = wide.astype(F32)
        square = square + jnp.sum(wide * wide, axis=1, keepdims=True)
    scale = lax.rsqrt(square * (1.0 / 2048.0) + EPS)
    for p in range(4):
        cols = pl.ds(512 * p, 512)
        nrm[:, cols] = (hid[:, cols].astype(F32) * scale * gain_ref[:, cols].astype(F32)).astype(BF16)

    tail = nrm[:, pl.ds(1536, 512)]
    for j in range(3):
        cols = pl.ds(512 * j, 512)
        packed = (dot(tmain[...], nrm[:, cols]) + dot(ttail[j], tail)).astype(BF16)
        outg[:, :, cols] = packed.reshape(16, 8, 512)
    disp = {}
    for d in range(1, 16):
        disp[d] = remote(outg.at[d], xbuf.at[0, d], disp_s.at[d], disp_r.at[d], sp_at(d))
        disp[d].start()
    xbuf[0, 0] = outg[0]

    def piece_at(buf, slot, piece):
        return buf.at[slot, pl.ds(4 * piece, 4)]

    def gather_hop(piece, way, hop):
        slot = GATHER[piece % 2][way][hop]
        to = (slot + 1) % 8 if way == 0 else (slot + 7) % 8
        c = remote(piece_at(xbuf, slot, piece), piece_at(xbuf, to, piece), ag_s.at[piece, to], ag_r.at[piece, to],
                   (right, left)[way])
        c.start()
        pending.append(c)

    def gather_wait(piece, slot):
        here = piece_at(xbuf, slot, piece)
        remote(here, here, ag_s.at[piece, slot], ag_r.at[piece, slot], right).wait_recv()

    def gather_start(pair):
        for piece in (2 * pair, 2 * pair + 1):
            for d in range(4 * piece, 4 * piece + 4):
                if d > 0:
                    disp[d].wait_recv()
            for way in range(2):
                gather_hop(piece, way, 0)

    def gather_tick(pair, k):
        for piece in (2 * pair, 2 * pair + 1):
            for way in range(2):
                slots = GATHER[piece % 2][way]
                if k <= len(slots):
                    gather_wait(piece, k if way == 0 else 8 - k)
                if k < len(slots):
                    gather_hop(piece, way, k)

    def expert(pair, slots):
        for i, slot in enumerate(slots):
            x2[pl.ds(64 * i, 64), pl.ds(0, 1536)] = xbuf[slot, pl.ds(8 * pair, 8)].reshape(64, 1536)
        tail = jnp.zeros((128, 512), F32)
        for j in range(3):
            tail = tail + dot(sel[j], x2[:, pl.ds(512 * j, 512)])
        x2[:, pl.ds(1536, 512)] = tail.astype(BF16)

        @pl.loop(0, 2)
        def _(h):
            gate = dot(x2[...], wg[h])
            up = dot(x2[...], wu[h])
            act[h] = (gate / (1.0 + jnp.exp(-gate)) * up).astype(BF16)

        def down(cols):
            return dot(act[0], wd[0, :, cols]) + dot(act[1], wd[1, :, cols])

        tail = down(pl.ds(1536, 512)).astype(BF16)
        low = lax.rem(lax.broadcasted_iota(jnp.int32, (128, 512), 0), 8) < 6

        @pl.loop(0, 3)
        def _(j):
            cols = pl.ds(pl.multiple_of(512 * j, 512), 512)
            packed = jnp.where(low, down(cols), dot(sel[3 + j], tail)).astype(BF16)
            for i, slot in enumerate(slots):
                part[slot, pl.ds(8 * pair, 8), :, cols] = packed[64 * i : 64 * i + 64].reshape(8, 8, 512)

    args = (
        lambda p, s: piece_at(part, s, p),
        lambda p, w, h: rbuf.at[p, w, h],
        rs_s,
        rs_r,
    )

    back = {}

    def send_back(pair):
        for piece in (2 * pair, 2 * pair + 1):
            total = reduce_last(piece, *args).astype(BF16)
            outg[pl.ds(4 * piece, 4)] = total
            for i in range(4):
                d = 4 * piece + i
                if d == 0:
                    ret[0] = total[0]
                else:
                    back[d] = remote(outg.at[d], ret.at[d], ret_s.at[d], ret_r.at[d], sp_at(16 - d))
                    back[d].start()
                    pending.append(back[d])

    gather_start(0)
    for c in local[1:]:
        c.wait()
    for c in e_duo:
        c.wait_recv()
    for k in (1, 2, 3):
        gather_tick(0, k)
        if k == 3:
            gather_start(1)
        expert(0, (k, 8 - k))
    gather_tick(0, 4)
    expert(0, (4, 0))
    for d in range(1, 16):
        disp[d].wait_send()
    for k in range(4):
        reduce_tick(k, (0, 1), *args)
        if k < 3:
            gather_tick(1, k + 1)
            expert(1, (k + 1, 7 - k))
        else:
            gather_tick(1, 4)
            expert(1, (4, 0))
    reduce_tick(0, (2, 3), *args)
    send_back(0)
    for k in range(1, 4):
        reduce_tick(k, (2, 3), *args)
    send_back(1)

    for d in range(1, 16):
        back[d].wait_recv()
    rw = rw_ref[...]
    weight = jnp.where(one[0], jnp.broadcast_to(rw[0:1, :], (128, 32)), 0.0) + jnp.where(
        one[1], jnp.broadcast_to(rw[1:2, :], (128, 32)), 0.0
    )
    parts = []
    for _ in range(3):
        parts.append(weight.astype(BF16))
        weight = weight - parts[-1].astype(F32)
    last = jnp.zeros((32, 512), F32)
    for j in range(3):
        cols = pl.ds(512 * j, 512)
        block = ret[:, :, cols].reshape(128, 512)
        acc = jnp.zeros((32, 512), F32)
        for w in parts:
            acc = acc + dot_t(w * tmain[...], block)
            last = last + dot_t(w * ttail[j], block)
        out_ref[:, cols] = (hid[:, cols].astype(F32) + acc).astype(BF16)
    cols = pl.ds(1536, 512)
    out_ref[:, cols] = (hid[:, cols].astype(F32) + last).astype(BF16)
    for c in pending:
        c.wait_send()


def shards(
    out_gate, in_gate, conv_input, conv_taps, documents, out_weight, residual, norm_gain, expert_ids, route_weights,
    gate_weight, up_weight, down_weight,
):
    vmem = pl.BlockSpec(memory_space=pltpu.VMEM)
    hbm = pl.BlockSpec(memory_space=pl.ANY)
    dma = pltpu.SemaphoreType.DMA
    scratch = [
        pltpu.VMEM((16, 128), BF16),
        pltpu.VMEM((16, 128), BF16),
        pltpu.VMEM((4, 128), jnp.int32),
        pltpu.VMEM((528, 128), F32),
        pltpu.VMEM((528, 128), F32),
        pltpu.VMEM((3, 256, 128), BF16),
        pltpu.VMEM((256, 256), BF16),
        pltpu.VMEM((2, 128, 2048), BF16),
        pltpu.VMEM((4, 8, 32, 512), BF16),
        pltpu.VMEM((4, 2, 4, 32, 512), BF16),
        pltpu.VMEM((32, 2048), BF16),
        pltpu.VMEM((32, 2048), BF16),
        pltpu.VMEM((128, 32), BF16),
        pltpu.VMEM((3, 128, 32), BF16),
        pltpu.VMEM((6, 128, 128), BF16),
        pltpu.VMEM((16, 8, 1536), BF16),
        pltpu.VMEM((8, 16, 8, 1536), BF16),
        pltpu.VMEM((128, 2048), BF16),
        pltpu.VMEM((2, 128, 256), BF16),
        pltpu.VMEM((2, 2048, 256), BF16),
        pltpu.VMEM((2, 2048, 256), BF16),
        pltpu.VMEM((2, 256, 2048), BF16),
        pltpu.VMEM((8, 16, 8, 1536), BF16),
        pltpu.VMEM((4, 2, 4, 4, 8, 1536), BF16),
        pltpu.VMEM((16, 8, 1536), BF16),
        dma((4,)),
        dma((3,)),
        dma((3,)),
        dma((5,)),
        dma((5,)),
        dma((4, 2, 4)),
        dma((4, 2, 4)),
        dma((16,)),
        dma((16,)),
        dma((4, 8)),
        dma((4, 8)),
        dma((4, 2, 4)),
        dma((4, 2, 4)),
        dma((16,)),
        dma((16,)),
    ]
    return pl.pallas_call(
        kernel,
        out_shape=jax.ShapeDtypeStruct((32, 2048), BF16),
        in_specs=[vmem] * 5 + [hbm] + [vmem] * 4 + [hbm] * 3,
        out_specs=vmem,
        scratch_shapes=scratch,
        compiler_params=pltpu.CompilerParams(
            collective_id=0, has_side_effects=True, vmem_limit_bytes=56 * 1024 * 1024
        ),
        name="layer",
    )(
        out_gate, in_gate, conv_input, conv_taps, documents.reshape(4, 128), out_weight, residual,
        norm_gain.reshape(1, 2048), expert_ids.T, route_weights.T, gate_weight, up_weight, down_weight,
    )


def solution(mesh):
    in_specs = (
        P("sp", "tp"),
        P("sp", "tp"),
        P("sp", "tp"),
        P(None, "tp"),
        P("sp"),
        P("tp", None),
        P(("sp", "tp"), None),
        P(),
        P(("sp", "tp"), None),
        P(("sp", "tp"), None),
        P("sp", None, "tp"),
        P("sp", None, "tp"),
        P("sp", "tp", None),
    )
    out_specs = P(("sp", "tp"), None)
    return jax.shard_map(shards, mesh=mesh, in_specs=in_specs, out_specs=out_specs, check_vma=False)
```

time: 252 us -> 114 us (0.45)
  waiting for transfers between devices: 166 us -> 0 us
  Pallas kernels: 0 us -> 110 us
  starting transfers between devices: 22.6 us -> 0 us
  matrix products: 21.6 us -> 0 us
  blocking collectives: 17.5 us -> 0 us
  between operations: 13.6 us -> 0.01 us
  other arithmetic: 5.69 us -> 0 us
    pallas_call x0 -> x1, Pallas kernels: none -> 110 us  [shards(): pl.pallas_call(kernel, out_shape=jax.ShapeDtypeStruct((32, 2048), BF16),...]
    reduce_scatter x1 -> x0, waiting for transfers between devices: 65.9 us -> none  [shards(): lax.psum_scatter(jnp.dot(act, down_weight[0], preferred_element_type=jnp....]
    all_to_all x2 -> x0, waiting for transfers between devices: 56.9 us -> none  [the longest x1 48.3 us: summed_on_arrival(): parts = lax.all_to_all(split_up(x, dim, count), axis, 0, 0, tiled=True)]
    all_gather x1 -> x0, waiting for transfers between devices: 42.1 us -> none  [shards(): gathered = lax.all_gather(arrived, 'tp', axis=0, tiled=True)]
    dot_general x4 -> x0, matrix products: 21.6 us -> none  [the longest x1 12.3 us: shards(): jnp.dot(act, down_weight[0], preferred_element_type=jnp.float32)]
    all_to_all x1 -> x0, blocking collectives: 17.5 us -> none  [shards(): lax.all_to_all(outgoing, 'sp', split_axis=0, concat_axis=0, tiled=True)]
    all_to_all x2 -> x0, starting transfers between devices: 16 us -> none  [the longest x1 8.7 us: summed_on_arrival(): parts = lax.all_to_all(split_up(x, dim, count), axis, 0, 0, tiled=True)]
    ppermute x2 -> x0, starting transfers between devices: 6.49 us -> none  [passed_along(): return lax.ppermute(block, axis, route)]
  transfers between devices with their start and end apart: 6 -> 0, of which waited for: 5 -> 0; matrix products, arithmetic and copies ran while one was open for 1% -> 0% of each run, Pallas kernels for 0% -> 0%
where the time goes in v1:
time: 114 us; the launch traced here: 113 us
  Pallas kernels  110 us (96%)
  local copies, waits for them, and re-layouts  2.86 us (3%)
    pallas_call x1, Pallas kernels, shards(): pl.pallas_call(kernel, out_shape=jax.ShapeDtypeStruct((32, 2048), BF16),...  110 us

profile of v1, /device:TPU:2, one launch (start us, length us, event | category | flops | bytes accessed | tf_op | source)
XLA Modules:
  0.0 112.8 jit_solution(8814505267384922733)
XLA Ops:
  0.0 0.0 copy-start
  0.0 0.7 copy-done
  0.7 0.6 reshape.7.gain_ref
  1.3 110.0 %layer.1 = bf16[32,2048]{1,0:T(8,128)(2,1)} custom-call(bf16[512,128]{1,0:T(8,128)(2,1)} %og_ref.1, bf16[512,128]{1,0:T(8,128)(2,1)} %ig_ref.1, bf16[512,128]{1,0:T(8,128)(2,1)} %ci_ref.1, bf16[3,128]{1,0:T(4,128)(2,1)} %taps_ref.1, s32[4,128]{1,0:T(4,128)} %bitcast.3, bf16[128,2048]{1,0:T(8,128)(2,1)} %ow_ref.1, bf16[32,2048]{1,0:T(8,128)(2,1)} %res_ref.1, ...), custom_call_target="tpu_custom_call" | custom-call | tf_op jit(solution)/shard_map/layer/pallas_call | solution.py:390
  111.3 1.6 %copy.15 = bf16[32,2048]{1,0:T(8,128)(2,1)} copy(bf16[32,2048]{1,0:T(8,128)(2,1)} %layer.1) | data formatting | bytes 262144
Async XLA Ops:
  0.0 0.7 copy-start

commit v2 on v1

v2 whole, which is shorter than its diff:
```python
import jax
import jax.numpy as jnp
from jax import lax
from jax.experimental import pallas as pl
from jax.experimental.pallas import tpu as pltpu
from jax.sharding import PartitionSpec as P

EPS = 1e-06
MESH = pl.DeviceIdType.MESH
F32 = jnp.float32
BF16 = jnp.bfloat16

GATHER = {0: ((0, 1, 2, 3), (0, 7, 6)), 1: ((0, 1, 2), (0, 7, 6, 5))}
REDUCE = {0: ((4, 5, 6, 7), (3, 2, 1)), 1: ((5, 6, 7), (4, 3, 2, 1))}
GROUPS = ((0, 1, 7, 2), (6, 3, 5, 4))
DY = (0, 2, 1, 3)
ORDER = (6, 5, 7, 4, 2, 1, 3, 10, 14, 9, 11, 13, 15, 8, 12)


def dot(a, b):
    return jnp.dot(a, b, preferred_element_type=F32)


def dot_t(a, b):
    return lax.dot_general(a, b, (((0,), (0,)), ((), ())), preferred_element_type=F32)


def iota(shape, dim):
    return lax.broadcasted_iota(jnp.int32, shape, dim)


def natural(q):
    d = (q * 2731) >> 16
    rest = q - 24 * d
    k = (rest * 10923) >> 16
    return d, k, rest - 6 * k


def kernel(
    og_hbm, ig_hbm, ci_hbm, taps_hbm, docs_hbm, ow_ref, res_hbm, gain_hbm, ids_hbm, rw_hbm, gw_ref, uw_ref, dw_ref,
    out_ref,
    og_ref, ig_ref, ci_ref, taps_ref, docs_ref, res_ref, gain_ref, ids_ref, rw_ref,
    h_ig, h_ci, h_docs, ext, extd, gbuf, xa, wa, part1, rbuf1, hid, nrm,
    line, meta, tmain, ttail, tdisp, tcomb, gm, gt, gmt, gtt,
    tok, outg, out2, xbuf, x2buf, xcat, x2, act, wg, wu, wd, part, rbuf, y2, back2, cpart, rbuf2, fin, ret,
    loc_sem, halo_s, halo_r, duo_s, duo_r, meta_s, meta_r, rs1_s, rs1_r, tok_s, tok_r, disp_s, disp_r, ag_s, ag_r,
    disp2_s, disp2_r, rs_s, rs_r, ret2_s, ret2_r, rs2_s, rs2_r, ret_s, ret_r,
):
    sp = lax.axis_index("sp")
    tp = lax.axis_index("tp")
    core = lax.rem(tp, 2)
    z = tp // 2
    y, x = sp // 4, lax.rem(sp, 4)
    right = {"tp": lax.rem(z + 1, 8) * 2 + core}
    left = {"tp": lax.rem(z + 7, 8) * 2 + core}
    sides = (right, left)
    partner = {"tp": z * 2 + 1 - core}
    following = {"sp": lax.rem(sp + 1, 16)}

    def ahead(d):
        return {"sp": lax.rem(y + DY[d // 4], 4) * 4 + lax.rem(x + d % 4, 4)}

    def behind(d):
        return {"sp": lax.rem(y + 4 - DY[d // 4], 4) * 4 + lax.rem(x + 4 - d % 4, 4)}

    def remote(src, dst, ssem, rsem, device):
        return pltpu.make_async_remote_copy(
            src_ref=src, dst_ref=dst, send_sem=ssem, recv_sem=rsem, device_id=device, device_id_type=MESH
        )

    pending = []

    def send(*args):
        c = remote(*args)
        c.start()
        pending.append(c)
        return c

    barrier = pltpu.get_barrier_semaphore()
    for device in [right, left, partner]:
        pl.semaphore_signal(barrier, inc=1, device_id=device, device_id_type=MESH)
    for d in range(1, 16):
        pl.semaphore_signal(barrier, inc=1, device_id=ahead(d), device_id_type=MESH)

    pairs = [
        (ids_hbm, ids_ref), (rw_hbm, rw_ref), (ig_hbm, ig_ref), (ci_hbm, ci_ref), (docs_hbm, docs_ref),
        (taps_hbm, taps_ref), (og_hbm, og_ref), (ow_ref, wa.at[0]), (res_hbm, res_ref), (gain_hbm, gain_ref),
        (gw_ref.at[0], wg.at[0]), (uw_ref.at[0], wu.at[0]), (dw_ref.at[0], wd.at[0]),
    ]
    local = [pltpu.make_async_copy(a, b, loc_sem.at[i]) for i, (a, b) in enumerate(pairs)]
    for c in local:
        c.start()

    local[0].wait()
    local[1].wait()
    ids = ids_ref[...]
    dy = ((ids >> 2) - y + 4) & 3
    rid = ((dy >> 1) + 2 * (dy & 1)) * 4 + (((ids & 3) - x + 4) & 3)
    weight = rw_ref[...]
    high = weight.astype(BF16).astype(F32)
    line[pl.ds(0, 2), :] = rid.astype(F32)
    line[pl.ds(2, 2), :] = high
    line[pl.ds(4, 2), :] = (weight - high).astype(BF16).astype(F32)
    line[pl.ds(6, 2), :] = jnp.zeros((2, 32), F32)
    spread = (iota((32, 128), 0) == (iota((32, 128), 1) & 31)).astype(BF16)
    meta[0] = dot(line[...].astype(BF16), spread)

    local[2].wait()
    local[3].wait()
    local[4].wait()
    local[5].wait()
    local[6].wait()
    ext[pl.ds(16, 512), :] = ig_ref[...].astype(F32) * ci_ref[...].astype(F32)
    docs = docs_ref[...].astype(F32)
    for i in range(4):
        extd[pl.ds(16 + 128 * i, 128), :] = jnp.broadcast_to(docs[i : i + 1, :], (128, 128)).T
    taps = taps_ref[...].astype(F32)

    def gated(first, count):
        pos = sp * 512 + first + iota((count, 128), 0)
        now = extd[pl.ds(16 + first, count), :]
        conv = taps[2:3, :] * ext[pl.ds(16 + first, count), :]
        for off in (1, 2):
            ok = (pos >= off) & (extd[pl.ds(16 + first - off, count), :] == now)
            earlier = taps[2 - off : 3 - off, :] * ext[pl.ds(16 + first - off, count), :]
            conv = conv + jnp.where(ok, earlier, 0.0)
        return (og_ref[pl.ds(first, count), :].astype(F32) * conv).astype(BF16)

    for j in range(1, 16):
        gbuf[j % 2, pl.ds(32 * (j // 2), 32), :] = gated(32 * j, 32)

    pl.semaphore_wait(barrier, 18)

    halo = [
        send(ig_hbm.at[pl.ds(496, 16)], h_ig, halo_s.at[0], halo_r.at[0], following),
        send(ci_hbm.at[pl.ds(496, 16)], h_ci, halo_s.at[1], halo_r.at[1], following),
        send(docs_hbm, h_docs, halo_s.at[2], halo_r.at[2], following),
    ]
    w_duo = send(ow_ref, wa.at[1], duo_s.at[0], duo_r.at[0], partner)

    def meta_tick(k):
        for way in range(2):
            slots = GATHER[0][way]
            if 0 < k <= len(slots):
                here = meta.at[k if way == 0 else 8 - k]
                sems = (meta_s.at[k if way == 0 else 8 - k], meta_r.at[k if way == 0 else 8 - k])
                remote(here, here, *sems, sides[way]).wait_recv()
            if k < len(slots):
                to = (slots[k] + 1) % 8 if way == 0 else (slots[k] + 7) % 8
                send(meta.at[slots[k]], meta.at[to], meta_s.at[to], meta_r.at[to], sides[way])

    meta_tick(0)
    for c in halo:
        c.wait_recv()
    ext[pl.ds(0, 16), :] = h_ig[...].astype(F32) * h_ci[...].astype(F32)
    old = jnp.broadcast_to(h_docs[...].astype(F32)[3:4, :], (128, 128)).T
    extd[pl.ds(0, 16), :] = old[112:128, :]
    gbuf[0, pl.ds(0, 32), :] = gated(0, 32)
    g_duo = send(gbuf.at[1 - core], gbuf.at[2], duo_s.at[1], duo_r.at[1], partner)
    xa[:, pl.ds(0, 128)] = gbuf[core]

    rows = iota((128, 32), 0)
    rel, sub = rows >> 3, (rows & 7).astype(F32)
    one = [(jnp.broadcast_to(rid[k : k + 1, :], (128, 32)) == rel) for k in range(2)]
    both = (one[0] | one[1]).astype(F32)
    before = (iota((32, 32), 0) < iota((32, 32), 1)).astype(BF16)
    place = dot(both.astype(BF16), before)
    tmain[...] = (jnp.where((place == sub) & (sub < 6.0), 1.0, 0.0) * both).astype(BF16)
    for j in range(3):
        hit = ((sub == 6.0) & (place == float(j))) | ((sub == 7.0) & (place == j + 3.0))
        ttail[j] = (jnp.where(hit, 1.0, 0.0) * both).astype(BF16)

    local[7].wait()
    w_duo.wait_recv()
    g_duo.wait_recv()
    xa[:, pl.ds(128, 128)] = gbuf[2]

    def reduce_hop(piece, way, hop, part_at, rbuf_at, ssem, rsem):
        slots = REDUCE[piece % 2][way]
        here = part_at(piece, slots[hop])
        if hop > 0:
            came = rbuf_at(piece, way, hop - 1)
            remote(came, came, ssem.at[piece, way, hop - 1], rsem.at[piece, way, hop - 1], sides[way]).wait_recv()
            here[...] = (here[...].astype(F32) + came[...].astype(F32)).astype(BF16)
        send(here, rbuf_at(piece, way, hop), ssem.at[piece, way, hop], rsem.at[piece, way, hop], sides[way])

    def reduce_tick(t, pieces, *rest):
        for piece in pieces:
            for way in range(2):
                hop = t - (4 - len(REDUCE[piece % 2][way]))
                if hop >= 0:
                    reduce_hop(piece, way, hop, *rest)

    def reduce_last(piece, part_at, rbuf_at, ssem, rsem):
        total = part_at(piece, 0)[...].astype(F32)
        for way in range(2):
            hop = len(REDUCE[piece % 2][way]) - 1
            here = rbuf_at(piece, way, hop)
            remote(here, here, ssem.at[piece, way, hop], rsem.at[piece, way, hop], sides[way]).wait_recv()
            total = total + here[...].astype(F32)
        return total

    args1 = (
        lambda p, s: part1.at[p, lax.rem(z - s + 8, 8)],
        lambda p, w, h: rbuf1.at[p, w, h],
        rs1_s,
        rs1_r,
    )
    for p in range(4):
        cols = pl.ds(512 * p, 512)
        prod = dot(xa[:, pl.ds(0, 128)], wa[0, :, cols]) + dot(xa[:, pl.ds(128, 128)], wa[1, :, cols])
        part1[p] = prod.astype(BF16).reshape(8, 32, 512)
        reduce_tick(0, (p,), *args1)
    e_duo = [
        send(gw_ref.at[0], wg.at[1], duo_s.at[2], duo_r.at[2], partner),
        send(uw_ref.at[0], wu.at[1], duo_s.at[3], duo_r.at[3], partner),
        send(dw_ref.at[0], wd.at[1], duo_s.at[4], duo_r.at[4], partner),
    ]

    def selections(axis, main, tails):
        shape = (192, 256) if axis == 0 else (256, 192)
        d, k, r = natural(iota(shape, axis))
        q = iota(shape, 1 - axis)
        same = (d == ((q >> 3) & 7)) & (k == (q >> 6))
        r8 = q & 7
        main[...] = jnp.where(same & (r8 == r), 1.0, 0.0).astype(BF16)
        for j in range(3):
            tails[j] = jnp.where(
                same & (((r8 == 6) & (r == j)) | ((r8 == 7) & (r == j + 3))), 1.0, 0.0
            ).astype(BF16)

    def tables(g):
        quarter = iota((8, 128), 1) >> 5
        m = jnp.zeros((8, 128), F32)
        for i, slot in enumerate(GROUPS[g]):
            m = jnp.where(quarter == i, meta[slot], m)
        d, k, r = natural(iota((384, 128), 0))
        lane = iota((384, 128), 1)
        d = d.astype(F32)
        first = jnp.broadcast_to(m[0:1, :], (384, 128)) == d
        second = jnp.broadcast_to(m[1:2, :], (384, 128)) == d
        named = (first | second).astype(F32)
        ta, tb = iota((128, 128), 0), iota((128, 128), 1)
        count = dot(named.astype(BF16), ((ta < tb) & ((ta >> 5) == (tb >> 5))).astype(BF16))
        table = jnp.where((count == r.astype(F32)) & (k == (lane >> 5)), named, 0.0)
        tdisp[g] = table.astype(BF16)
        for i in range(2):
            w = jnp.where(first, m[2 + 2 * i : 3 + 2 * i, :], m[3 + 2 * i : 4 + 2 * i, :])
            tcomb[g, i] = (table * w).astype(BF16)

    meta_tick(1)
    selections(0, gm, gt)
    reduce_tick(1, range(4), *args1)
    meta_tick(2)
    tables(0)
    reduce_tick(2, range(4), *args1)
    meta_tick(3)
    selections(1, gmt, gtt)
    reduce_tick(3, range(4), *args1)
    meta_tick(4)
    local[8].wait()
    local[9].wait()
    square = jnp.zeros((32, 1), F32)
    for p in range(4):
        cols = pl.ds(512 * p, 512)
        wide = (res_ref[:, cols].astype(F32) + reduce_last(p, *args1)).astype(BF16)
        hid[:, cols] = wide
        wide = wide.astype(F32)
        square = square + jnp.sum(wide * wide, axis=1, keepdims=True)
    scale = lax.rsqrt(square * (1.0 / 2048.0) + EPS)
    gain = gain_ref[...].astype(F32)
    for i in list(range(8, 16)) + list(range(8)):
        cols = pl.ds(128 * i, 128)
        nrm[:, cols] = (hid[:, cols].astype(F32) * scale * gain[i : i + 1, :]).astype(BF16)
    for c in range(2):
        tok[c, 0] = nrm[:, pl.ds(1024 + 512 * c, 512)]

    def tok_tick(k):
        for c in range(2):
            for way in range(2):
                slots = GATHER[c][way]
                if 0 < k <= len(slots):
                    slot = k if way == 0 else 8 - k
                    here = tok.at[c, slot]
                    remote(here, here, tok_s.at[c, slot], tok_r.at[c, slot], sides[way]).wait_recv()
                if k < len(slots):
                    to = (slots[k] + 1) % 8 if way == 0 else (slots[k] + 7) % 8
                    send(tok.at[c, slots[k]], tok.at[c, to], tok_s.at[c, to], tok_r.at[c, to], sides[way])

    tok_tick(0)

    tail = nrm[:, pl.ds(768, 256)]
    for j in range(3):
        cols = pl.ds(256 * j, 256)
        packed = (dot(tmain[...], nrm[:, cols]) + dot(ttail[j], tail)).astype(BF16)
        outg[:, :, cols] = packed.reshape(16, 8, 256)
    disp = {d: send(outg.at[d], xbuf.at[0, d], disp_s.at[d], disp_r.at[d], ahead(d)) for d in ORDER}
    xbuf[0, 0] = outg[0]

    def disp2(g):
        for c in range(2):
            cols = pl.ds(512 * c, 512)
            block = jnp.concatenate([tok[c, slot] for slot in GROUPS[g]], axis=0)
            out2[g, :, :, cols] = dot(tdisp[g], block).astype(BF16).reshape(16, 24, 512)
        for d in ORDER:
            came[g, d] = send(out2.at[g, d], x2buf.at[g, d], disp2_s.at[g, d], disp2_r.at[g, d], ahead(d))
        x2buf[g, 0] = out2[g, 0]

    came = {}

    def piece_at(buf, slot, piece):
        return buf.at[slot, pl.ds(4 * piece, 4)]

    def gather_tick(pair, k):
        for piece in (2 * pair, 2 * pair + 1):
            if k == 0:
                for d in range(4 * piece, 4 * piece + 4):
                    if d > 0:
                        disp[d].wait_recv()
            for way in range(2):
                slots = GATHER[piece % 2][way]
                if 0 < k <= len(slots):
                    slot = k if way == 0 else 8 - k
                    here = piece_at(xbuf, slot, piece)
                    remote(here, here, ag_s.at[piece, slot], ag_r.at[piece, slot], sides[way]).wait_recv()
                if k < len(slots):
                    to = (slots[k] + 1) % 8 if way == 0 else (slots[k] + 7) % 8
                    send(piece_at(xbuf, slots[k], piece), piece_at(xbuf, to, piece), ag_s.at[piece, to],
                         ag_r.at[piece, to], sides[way])

    def expert(pair, g):
        these = pl.ds(8 * pair, 8)
        for d in range(8 * pair, 8 * pair + 8):
            if d > 0:
                came[g, d].wait_recv()
        for i, slot in enumerate(GROUPS[g]):
            xcat[pl.ds(64 * i, 64), :] = xbuf[slot, these].reshape(64, 768)
        x2[:, pl.ds(0, 768)] = dot(gm[...], xcat[...]).astype(BF16)
        last = jnp.zeros((192, 256), F32)
        for j in range(3):
            last = last + dot(gt[j], xcat[:, pl.ds(256 * j, 256)])
        x2[:, pl.ds(768, 256)] = last.astype(BF16)
        x2[:, pl.ds(1024, 1024)] = x2buf[g, these].reshape(192, 1024)

        @pl.loop(0, 2)
        def _(h):
            gate = dot(x2[...], wg[h])
            up = dot(x2[...], wu[h])
            act[h] = (gate / (1.0 + jnp.exp(-gate)) * up).astype(BF16)

        def down(cols):
            return (dot(act[0], wd[0, :, cols]) + dot(act[1], wd[1, :, cols])).astype(BF16)

        @pl.loop(0, 2)
        def _(c):
            cols = pl.ds(pl.multiple_of(512 * c, 512), 512)
            y2[g, these, :, cols] = down(pl.ds(pl.multiple_of(1024 + 512 * c, 512), 512)).reshape(8, 24, 512)

        for d in ORDER:
            if d // 8 == pair:
                home[g, d] = send(y2.at[g, d], back2.at[g, d], ret2_s.at[g, d], ret2_r.at[g, d], behind(d))
        if pair == 0:
            back2[g, 0] = y2[g, 0]
        last = down(pl.ds(768, 256))

        @pl.loop(0, 3)
        def _(j):
            cols = pl.ds(pl.multiple_of(256 * j, 256), 256)
            packed = (dot(gmt[...], down(cols)) + dot(gtt[j], last)).astype(BF16)
            for i, slot in enumerate(GROUPS[g]):
                part[slot, these, :, cols] = packed[64 * i : 64 * i + 64].reshape(8, 8, 256)

    home = {}
    args = (
        lambda p, s: piece_at(part, s, p),
        lambda p, w, h: rbuf.at[p, w, h],
        rs_s,
        rs_r,
    )
    back = {}

    def send_back(pair):
        for piece in (2 * pair, 2 * pair + 1):
            fin[pl.ds(4 * piece, 4)] = reduce_last(piece, *args).astype(BF16)
            for d in range(4 * piece, 4 * piece + 4):
                if d == 0:
                    ret[0] = fin[0]
                else:
                    back[d] = send(fin.at[d], ret.at[d], ret_s.at[d], ret_r.at[d], behind(d))

    args2 = (
        lambda p, s: cpart.at[p, s],
        lambda p, w, h: rbuf2.at[p, w, h],
        rs2_s,
        rs2_r,
    )

    def combine(g):
        for d in range(1, 16):
            home[g, d].wait_recv()
        for c in range(2):
            block = back2[g, :, :, pl.ds(512 * c, 512)].reshape(384, 512)
            total = dot_t(tcomb[g, 0], block) + dot_t(tcomb[g, 1], block)
            for i, slot in enumerate(GROUPS[g]):
                cpart[c, slot] = total[32 * i : 32 * i + 32].astype(BF16)

    tables(1)
    tok_tick(1)
    gather_tick(0, 0)
    tok_tick(2)
    disp2(0)
    gather_tick(0, 1)
    tok_tick(3)
    gather_tick(0, 2)
    gather_tick(1, 0)
    tok_tick(4)
    disp2(1)
    gather_tick(0, 3)
    gather_tick(1, 1)
    for c in local[10:]:
        c.wait()
    for c in e_duo:
        c.wait_recv()
    expert(0, 0)
    gather_tick(0, 4)
    gather_tick(1, 2)
    gather_tick(1, 3)
    expert(0, 1)
    reduce_tick(0, (0, 1), *args)
    gather_tick(1, 4)
    reduce_tick(1, (0, 1), *args)
    expert(1, 1)
    reduce_tick(0, (2, 3), *args)
    reduce_tick(2, (0, 1), *args)
    expert(1, 0)
    reduce_tick(1, (2, 3), *args)
    reduce_tick(3, (0, 1), *args)
    combine(1)
    reduce_tick(0, (0, 1), *args2)
    reduce_tick(2, (2, 3), *args)
    send_back(0)
    reduce_tick(1, (0, 1), *args2)
    combine(0)
    reduce_tick(3, (2, 3), *args)
    reduce_tick(2, (0, 1), *args2)
    send_back(1)
    reduce_tick(3, (0, 1), *args2)

    for c in range(2):
        cols = pl.ds(1024 + 512 * c, 512)
        out_ref[:, cols] = (hid[:, cols].astype(F32) + reduce_last(c, *args2)).astype(BF16)
    for d in range(1, 16):
        back[d].wait_recv()
    weight = [
        jnp.where(one[0], line[i : i + 1, :], 0.0) + jnp.where(one[1], line[i + 1 : i + 2, :], 0.0) for i in (2, 4)
    ]
    weight = [w.astype(BF16) for w in weight]
    last = jnp.zeros((32, 256), F32)
    for j in range(3):
        cols = pl.ds(256 * j, 256)
        block = ret[:, :, cols].reshape(128, 256)
        acc = jnp.zeros((32, 256), F32)
        for w in weight:
            acc = acc + dot_t(w * tmain[...], block)
            last = last + dot_t(w * ttail[j], block)
        out_ref[:, cols] = (hid[:, cols].astype(F32) + acc).astype(BF16)
    cols = pl.ds(768, 256)
    out_ref[:, cols] = (hid[:, cols].astype(F32) + last).astype(BF16)
    for c in pending:
        c.wait_send()


def shards(
    out_gate, in_gate, conv_input, conv_taps, documents, out_weight, residual, norm_gain, expert_ids, route_weights,
    gate_weight, up_weight, down_weight,
):
    hbm = pl.BlockSpec(memory_space=pl.ANY)
    dma = pltpu.SemaphoreType.DMA

    def buf(*shape, dtype=BF16):
        return pltpu.VMEM(shape, dtype)

    scratch = [
        buf(512, 128), buf(512, 128), buf(512, 128), buf(3, 128), buf(4, 128, dtype=jnp.int32), buf(32, 2048),
        buf(16, 128), buf(2, 32, dtype=jnp.int32), buf(2, 32, dtype=F32),
        buf(16, 128), buf(16, 128), buf(4, 128, dtype=jnp.int32), buf(528, 128, dtype=F32), buf(528, 128, dtype=F32),
        buf(3, 256, 128), buf(256, 256), buf(2, 128, 2048), buf(4, 8, 32, 512), buf(4, 2, 4, 32, 512),
        buf(32, 2048), buf(32, 2048),
        buf(8, 32, dtype=F32), buf(8, 8, 128, dtype=F32), buf(128, 32), buf(3, 128, 32), buf(2, 384, 128),
        buf(2, 2, 384, 128), buf(192, 256), buf(3, 192, 256), buf(256, 192), buf(3, 256, 192),
        buf(2, 8, 32, 512), buf(16, 8, 768), buf(2, 16, 24, 1024), buf(8, 16, 8, 768), buf(2, 16, 24, 1024),
        buf(256, 768), buf(192, 2048), buf(2, 192, 256), buf(2, 2048, 256), buf(2, 2048, 256), buf(2, 256, 2048),
        buf(8, 16, 8, 768), buf(4, 2, 4, 4, 8, 768), buf(2, 16, 24, 1024), buf(2, 16, 24, 1024), buf(2, 8, 32, 512),
        buf(2, 2, 4, 32, 512), buf(16, 8, 768), buf(16, 8, 768),
        dma((13,)), dma((3,)), dma((3,)), dma((5,)), dma((5,)), dma((8,)), dma((8,)), dma((4, 2, 4)), dma((4, 2, 4)),
        dma((2, 8)), dma((2, 8)), dma((16,)), dma((16,)), dma((4, 8)), dma((4, 8)),
        dma((2, 16)), dma((2, 16)), dma((4, 2, 4)), dma((4, 2, 4)), dma((2, 16)), dma((2, 16)), dma((2, 2, 4)),
        dma((2, 2, 4)), dma((16,)), dma((16,)),
    ]
    return pl.pallas_call(
        kernel,
        out_shape=jax.ShapeDtypeStruct((32, 2048), BF16),
        in_specs=[hbm] * 13,
        out_specs=pl.BlockSpec(memory_space=pltpu.VMEM),
        scratch_shapes=scratch,
        compiler_params=pltpu.CompilerParams(
            collective_id=0, has_side_effects=True, vmem_limit_bytes=56 * 1024 * 1024
        ),
        name="layer",
    )(
        out_gate, in_gate, conv_input, conv_taps, documents.reshape(4, 128), out_weight, residual,
        norm_gain.reshape(16, 128), expert_ids.T, route_weights.T, gate_weight, up_weight, down_weight,
    )


def solution(mesh):
    in_specs = (
        P("sp", "tp"),
        P("sp", "tp"),
        P("sp", "tp"),
        P(None, "tp"),
        P("sp"),
        P("tp", None),
        P(("sp", "tp"), None),
        P(),
        P(("sp", "tp"), None),
        P(("sp", "tp"), None),
        P("sp", None, "tp"),
        P("sp", None, "tp"),
        P("sp", "tp", None),
    )
    out_specs = P(("sp", "tp"), None)
    return jax.shard_map(shards, mesh=mesh, in_specs=in_specs, out_specs=out_specs, check_vma=False)
```

time: 114 us -> 97 us (0.85)
  Pallas kernels: 110 us -> 94.6 us
  local copies, waits for them, and re-layouts: 2.86 us -> 1.57 us
    pallas_call x1, Pallas kernels: 110 us -> 94.6 us  [shards(): pl.pallas_call(kernel, out_shape=jax.ShapeDtypeStruct((32, 2048), BF16),...]
where the time goes in v2:
time: 97 us; the launch traced here: 96.2 us
  Pallas kernels  94.6 us (98%)
  local copies, waits for them, and re-layouts  1.57 us (2%)
    pallas_call x1, Pallas kernels, shards(): pl.pallas_call(kernel, out_shape=jax.ShapeDtypeStruct((32, 2048), BF16),...  94.6 us

profile of v2, /device:TPU:2, one launch (start us, length us, event | category | flops | bytes accessed | tf_op | source)
XLA Modules:
  0.0 96.2 jit_solution(14883725311675110610)
XLA Ops:
  0.0 94.6 %layer.1 = bf16[32,2048]{1,0:T(8,128)(2,1)} custom-call(bf16[512,128]{1,0:T(8,128)(2,1)} %og_hbm.1, bf16[512,128]{1,0:T(8,128)(2,1)} %ig_hbm.1, bf16[512,128]{1,0:T(8,128)(2,1)} %ci_hbm.1, bf16[3,128]{1,0:T(4,128)(2,1)} %taps_hbm.1, s32[4,128]{1,0:T(4,128)} %bitcast.5, bf16[128,2048]{1,0:T(8,128)(2,1)} %ow_ref.1, bf16[32,2048]{1,0:T(8,128)(2,1)} %res_hbm.1, ...), custom_call_target="tpu_custom_call" | custom-call | tf_op jit(solution)/shard_map/layer/pallas_call | solution.py:500
  94.7 1.6 %copy.15 = bf16[32,2048]{1,0:T(8,128)(2,1)} copy(bf16[32,2048]{1,0:T(8,128)(2,1)} %layer.1) | data formatting | bytes 262144

commit v3 on v2

--- a/solution.py
+++ b/solution.py
@@ -40,11 +40,10 @@
     og_hbm, ig_hbm, ci_hbm, taps_hbm, docs_hbm, ow_ref, res_hbm, gain_hbm, ids_hbm, rw_hbm, gw_ref, uw_ref, dw_ref,
     out_ref,
     og_ref, ig_ref, ci_ref, taps_ref, docs_ref, res_ref, gain_ref, ids_ref, rw_ref,
-    h_ig, h_ci, h_docs, ext, extd, gbuf, xa, wa, part1, rbuf1, hid, nrm,
+    h_in, h_docs, ext, extd, gbuf, xa, wa, part1, rbuf1, hid, nrm,
     line, meta, tmain, ttail, tdisp, tcomb, gm, gt, gmt, gtt,
     tok, outg, out2, xbuf, x2buf, xcat, x2, act, wg, wu, wd, part, rbuf, y2, back2, cpart, rbuf2, fin, ret,
-    loc_sem, halo_s, halo_r, duo_s, duo_r, meta_s, meta_r, rs1_s, rs1_r, tok_s, tok_r, disp_s, disp_r, ag_s, ag_r,
-    disp2_s, disp2_r, rs_s, rs_r, ret2_s, ret2_r, rs2_s, rs2_r, ret_s, ret_r,
+    loc_sem, out_sem, in_sem, meta_r, ag_r, rs_r, tok_r, ret_r,
 ):
     sp = lax.axis_index("sp")
     tp = lax.axis_index("tp")
@@ -68,13 +67,16 @@
             src_ref=src, dst_ref=dst, send_sem=ssem, recv_sem=rsem, device_id=device, device_id_type=MESH
         )
 
-    pending = []
-
     def send(*args):
         c = remote(*args)
         c.start()
-        pending.append(c)
         return c
+
+    def sent(ref, i):
+        remote(ref, ref, out_sem.at[i], in_sem.at[0], right).wait_send()
+
+    def received(ref, sem):
+        remote(ref, ref, out_sem.at[0], sem, right).wait_recv()
 
     barrier = pltpu.get_barrier_semaphore()
     for device in [right, left, partner]:
@@ -131,32 +133,39 @@
 
     pl.semaphore_wait(barrier, 18)
 
-    halo = [
-        send(ig_hbm.at[pl.ds(496, 16)], h_ig, halo_s.at[0], halo_r.at[0], following),
-        send(ci_hbm.at[pl.ds(496, 16)], h_ci, halo_s.at[1], halo_r.at[1], following),
-        send(docs_hbm, h_docs, halo_s.at[2], halo_r.at[2], following),
+    send(ig_ref.at[pl.ds(496, 16)], h_in.at[0], out_sem.at[0], in_sem.at[0], following)
+    send(ci_ref.at[pl.ds(496, 16)], h_in.at[1], out_sem.at[0], in_sem.at[0], following)
+    send(docs_ref, h_docs, out_sem.at[1], in_sem.at[1], following)
+    rest = pl.ds(32, 224)
+    g_duo = [send(gbuf.at[1 - core, rest], gbuf.at[2, rest], out_sem.at[2], in_sem.at[2], partner)]
+    local[7].wait()
+    w_duo = send(wa.at[0], wa.at[1], out_sem.at[3], in_sem.at[3], partner)
+
+    e_duo = [
+        send(gw_ref.at[0], wg.at[1], out_sem.at[7], in_sem.at[5], partner),
+        send(uw_ref.at[0], wu.at[1], out_sem.at[8], in_sem.at[6], partner),
     ]
-    w_duo = send(ow_ref, wa.at[1], duo_s.at[0], duo_r.at[0], partner)
 
     def meta_tick(k):
         for way in range(2):
             slots = GATHER[0][way]
             if 0 < k <= len(slots):
-                here = meta.at[k if way == 0 else 8 - k]
-                sems = (meta_s.at[k if way == 0 else 8 - k], meta_r.at[k if way == 0 else 8 - k])
-                remote(here, here, *sems, sides[way]).wait_recv()
+                slot = k if way == 0 else 8 - k
+                received(meta.at[slot], meta_r.at[slot - 1])
             if k < len(slots):
                 to = (slots[k] + 1) % 8 if way == 0 else (slots[k] + 7) % 8
-                send(meta.at[slots[k]], meta.at[to], meta_s.at[to], meta_r.at[to], sides[way])
+                send(meta.at[slots[k]], meta.at[to], out_sem.at[4], meta_r.at[to - 1], sides[way])
 
     meta_tick(0)
-    for c in halo:
-        c.wait_recv()
-    ext[pl.ds(0, 16), :] = h_ig[...].astype(F32) * h_ci[...].astype(F32)
+    received(h_in, in_sem.at[0])
+    received(h_docs, in_sem.at[1])
+    ext[pl.ds(0, 16), :] = h_in[0].astype(F32) * h_in[1].astype(F32)
     old = jnp.broadcast_to(h_docs[...].astype(F32)[3:4, :], (128, 128)).T
     extd[pl.ds(0, 16), :] = old[112:128, :]
     gbuf[0, pl.ds(0, 32), :] = gated(0, 32)
-    g_duo = send(gbuf.at[1 - core], gbuf.at[2], duo_s.at[1], duo_r.at[1], partner)
+    rest = pl.ds(0, 32)
+    g_duo.append(send(gbuf.at[1 - core, rest], gbuf.at[2, rest], out_sem.at[5], in_sem.at[4], partner))
+    e_duo.append(send(dw_ref.at[0], wd.at[1], out_sem.at[9], in_sem.at[7], partner))
     xa[:, pl.ds(0, 128)] = gbuf[core]
 
     rows = iota((128, 32), 0)
@@ -170,19 +179,22 @@
         hit = ((sub == 6.0) & (place == float(j))) | ((sub == 7.0) & (place == j + 3.0))
         ttail[j] = (jnp.where(hit, 1.0, 0.0) * both).astype(BF16)
 
-    local[7].wait()
     w_duo.wait_recv()
-    g_duo.wait_recv()
+    for c in g_duo:
+        c.wait_recv()
     xa[:, pl.ds(128, 128)] = gbuf[2]
+
+    def arrival(rsem, piece, way, hop):
+        return rsem.at[piece, hop if way == 0 else len(REDUCE[piece % 2][0]) + hop]
 
     def reduce_hop(piece, way, hop, part_at, rbuf_at, ssem, rsem):
         slots = REDUCE[piece % 2][way]
         here = part_at(piece, slots[hop])
         if hop > 0:
             came = rbuf_at(piece, way, hop - 1)
-            remote(came, came, ssem.at[piece, way, hop - 1], rsem.at[piece, way, hop - 1], sides[way]).wait_recv()
+            received(came, arrival(rsem, piece, way, hop - 1))
             here[...] = (here[...].astype(F32) + came[...].astype(F32)).astype(BF16)
-        send(here, rbuf_at(piece, way, hop), ssem.at[piece, way, hop], rsem.at[piece, way, hop], sides[way])
+        send(here, rbuf_at(piece, way, hop), ssem, arrival(rsem, piece, way, hop), sides[way])
 
     def reduce_tick(t, pieces, *rest):
         for piece in pieces:
@@ -196,27 +208,21 @@
         for way in range(2):
             hop = len(REDUCE[piece % 2][way]) - 1
             here = rbuf_at(piece, way, hop)
-            remote(here, here, ssem.at[piece, way, hop], rsem.at[piece, way, hop], sides[way]).wait_recv()
+            received(here, arrival(rsem, piece, way, hop))
             total = total + here[...].astype(F32)
         return total
 
     args1 = (
         lambda p, s: part1.at[p, lax.rem(z - s + 8, 8)],
         lambda p, w, h: rbuf1.at[p, w, h],
-        rs1_s,
-        rs1_r,
+        out_sem.at[6],
+        rs_r,
     )
     for p in range(4):
         cols = pl.ds(512 * p, 512)
         prod = dot(xa[:, pl.ds(0, 128)], wa[0, :, cols]) + dot(xa[:, pl.ds(128, 128)], wa[1, :, cols])
         part1[p] = prod.astype(BF16).reshape(8, 32, 512)
         reduce_tick(0, (p,), *args1)
-    e_duo = [
-        send(gw_ref.at[0], wg.at[1], duo_s.at[2], duo_r.at[2], partner),
-        send(uw_ref.at[0], wu.at[1], duo_s.at[3], duo_r.at[3], partner),
-        send(dw_ref.at[0], wd.at[1], duo_s.at[4], duo_r.at[4], partner),
-    ]
-
     def selections(axis, main, tails):
         shape = (192, 256) if axis == 0 else (256, 192)
         d, k, r = natural(iota(shape, axis))
@@ -281,11 +287,10 @@
                 slots = GATHER[c][way]
                 if 0 < k <= len(slots):
                     slot = k if way == 0 else 8 - k
-                    here = tok.at[c, slot]
-                    remote(here, here, tok_s.at[c, slot], tok_r.at[c, slot], sides[way]).wait_recv()
+                    received(tok.at[c, slot], tok_r.at[c, slot - 1])
                 if k < len(slots):
                     to = (slots[k] + 1) % 8 if way == 0 else (slots[k] + 7) % 8
-                    send(tok.at[c, slots[k]], tok.at[c, to], tok_s.at[c, to], tok_r.at[c, to], sides[way])
+                    send(tok.at[c, slots[k]], tok.at[c, to], out_sem.at[10], tok_r.at[c, to - 1], sides[way])
 
     tok_tick(0)
 
@@ -294,7 +299,8 @@
         cols = pl.ds(256 * j, 256)
         packed = (dot(tmain[...], nrm[:, cols]) + dot(ttail[j], tail)).astype(BF16)
         outg[:, :, cols] = packed.reshape(16, 8, 256)
-    disp = {d: send(outg.at[d], xbuf.at[0, d], disp_s.at[d], disp_r.at[d], ahead(d)) for d in ORDER}
+    for d in ORDER:
+        send(outg.at[d], xbuf.at[0, d], out_sem.at[11], in_sem.at[8 + d // 8], ahead(d))
     xbuf[0, 0] = outg[0]
 
     def disp2(g):
@@ -303,81 +309,72 @@
             block = jnp.concatenate([tok[c, slot] for slot in GROUPS[g]], axis=0)
             out2[g, :, :, cols] = dot(tdisp[g], block).astype(BF16).reshape(16, 24, 512)
         for d in ORDER:
-            came[g, d] = send(out2.at[g, d], x2buf.at[g, d], disp2_s.at[g, d], disp2_r.at[g, d], ahead(d))
+            send(out2.at[g, d], x2buf.at[g, d], out_sem.at[12 + g], in_sem.at[10 + 2 * g + d // 8], ahead(d))
         x2buf[g, 0] = out2[g, 0]
-
-    came = {}
 
     def piece_at(buf, slot, piece):
         return buf.at[slot, pl.ds(4 * piece, 4)]
 
+    def whole(pair):
+        return pl.ds(8, 8) if pair else pl.ds(1, 7)
+
     def gather_tick(pair, k):
+        if k == 0:
+            received(xbuf.at[0, whole(pair)], in_sem.at[8 + pair])
         for piece in (2 * pair, 2 * pair + 1):
-            if k == 0:
-                for d in range(4 * piece, 4 * piece + 4):
-                    if d > 0:
-                        disp[d].wait_recv()
             for way in range(2):
                 slots = GATHER[piece % 2][way]
                 if 0 < k <= len(slots):
                     slot = k if way == 0 else 8 - k
-                    here = piece_at(xbuf, slot, piece)
-                    remote(here, here, ag_s.at[piece, slot], ag_r.at[piece, slot], sides[way]).wait_recv()
+                    received(piece_at(xbuf, slot, piece), ag_r.at[piece, slot - 1])
                 if k < len(slots):
                     to = (slots[k] + 1) % 8 if way == 0 else (slots[k] + 7) % 8
-                    send(piece_at(xbuf, slots[k], piece), piece_at(xbuf, to, piece), ag_s.at[piece, to],
-                         ag_r.at[piece, to], sides[way])
-
-    def expert(pair, g):
+                    send(piece_at(xbuf, slots[k], piece), piece_at(xbuf, to, piece), out_sem.at[14],
+                         ag_r.at[piece, to - 1], sides[way])
+
+    def expert(pair, g, step):
         these = pl.ds(8 * pair, 8)
-        for d in range(8 * pair, 8 * pair + 8):
-            if d > 0:
-                came[g, d].wait_recv()
-        for i, slot in enumerate(GROUPS[g]):
-            xcat[pl.ds(64 * i, 64), :] = xbuf[slot, these].reshape(64, 768)
-        x2[:, pl.ds(0, 768)] = dot(gm[...], xcat[...]).astype(BF16)
-        last = jnp.zeros((192, 256), F32)
-        for j in range(3):
-            last = last + dot(gt[j], xcat[:, pl.ds(256 * j, 256)])
-        x2[:, pl.ds(768, 256)] = last.astype(BF16)
-        x2[:, pl.ds(1024, 1024)] = x2buf[g, these].reshape(192, 1024)
-
-        @pl.loop(0, 2)
-        def _(h):
-            gate = dot(x2[...], wg[h])
-            up = dot(x2[...], wu[h])
-            act[h] = (gate / (1.0 + jnp.exp(-gate)) * up).astype(BF16)
 
         def down(cols):
             return (dot(act[0], wd[0, :, cols]) + dot(act[1], wd[1, :, cols])).astype(BF16)
 
-        @pl.loop(0, 2)
-        def _(c):
-            cols = pl.ds(pl.multiple_of(512 * c, 512), 512)
-            y2[g, these, :, cols] = down(pl.ds(pl.multiple_of(1024 + 512 * c, 512), 512)).reshape(8, 24, 512)
-
-        for d in ORDER:
-            if d // 8 == pair:
-                home[g, d] = send(y2.at[g, d], back2.at[g, d], ret2_s.at[g, d], ret2_r.at[g, d], behind(d))
-        if pair == 0:
-            back2[g, 0] = y2[g, 0]
-        last = down(pl.ds(768, 256))
-
-        @pl.loop(0, 3)
-        def _(j):
-            cols = pl.ds(pl.multiple_of(256 * j, 256), 256)
-            packed = (dot(gmt[...], down(cols)) + dot(gtt[j], last)).astype(BF16)
+        if step == 0:
             for i, slot in enumerate(GROUPS[g]):
-                part[slot, these, :, cols] = packed[64 * i : 64 * i + 64].reshape(8, 8, 256)
-
-    home = {}
+                xcat[pl.ds(64 * i, 64), :] = xbuf[slot, these].reshape(64, 768)
+            x2[:, pl.ds(0, 768)] = dot(gm[...], xcat[...]).astype(BF16)
+            last = jnp.zeros((192, 256), F32)
+            for j in range(3):
+                last = last + dot(gt[j], xcat[:, pl.ds(256 * j, 256)])
+            x2[:, pl.ds(768, 256)] = last.astype(BF16)
+            received(x2buf.at[g, whole(pair)], in_sem.at[10 + 2 * g + pair])
+            x2[:, pl.ds(1024, 1024)] = x2buf[g, these].reshape(192, 1024)
+        if step < 2:
+            gate = dot(x2[...], wg[step])
+            up = dot(x2[...], wu[step])
+            act[step] = (gate / (1.0 + jnp.exp(-gate)) * up).astype(BF16)
+        if step == 2:
+            for c in range(2):
+                y2[g, these, :, pl.ds(512 * c, 512)] = down(pl.ds(1024 + 512 * c, 512)).reshape(8, 24, 512)
+
+            for d in ORDER:
+                if d // 8 == pair:
+                    send(y2.at[g, d], back2.at[g, d], out_sem.at[15], in_sem.at[14 + g], behind(d))
+            if pair == 0:
+                back2[g, 0] = y2[g, 0]
+        if step == 3:
+            last = down(pl.ds(768, 256))
+            for j in range(3):
+                cols = pl.ds(256 * j, 256)
+                packed = (dot(gmt[...], down(cols)) + dot(gtt[j], last)).astype(BF16)
+                for i, slot in enumerate(GROUPS[g]):
+                    part[slot, these, :, cols] = packed[64 * i : 64 * i + 64].reshape(8, 8, 256)
+
     args = (
         lambda p, s: piece_at(part, s, p),
         lambda p, w, h: rbuf.at[p, w, h],
-        rs_s,
+        out_sem.at[16],
         rs_r,
     )
-    back = {}
 
     def send_back(pair):
         for piece in (2 * pair, 2 * pair + 1):
@@ -386,18 +383,17 @@
                 if d == 0:
                     ret[0] = fin[0]
                 else:
-                    back[d] = send(fin.at[d], ret.at[d], ret_s.at[d], ret_r.at[d], behind(d))
+                    send(fin.at[d], ret.at[d], out_sem.at[17], ret_r, behind(d))
 
     args2 = (
         lambda p, s: cpart.at[p, s],
         lambda p, w, h: rbuf2.at[p, w, h],
-        rs2_s,
-        rs2_r,
+        out_sem.at[18],
+        tok_r,
     )
 
     def combine(g):
-        for d in range(1, 16):
-            home[g, d].wait_recv()
+        received(back2.at[g, pl.ds(1, 15)], in_sem.at[14 + g])
         for c in range(2):
             block = back2[g, :, :, pl.ds(512 * c, 512)].reshape(384, 512)
             total = dot_t(tcomb[g, 0], block) + dot_t(tcomb[g, 1], block)
@@ -415,32 +411,44 @@
     gather_tick(1, 0)
     tok_tick(4)
     disp2(1)
-    gather_tick(0, 3)
-    gather_tick(1, 1)
     for c in local[10:]:
         c.wait()
     for c in e_duo:
         c.wait_recv()
-    expert(0, 0)
+    expert(0, 0, 0)
+    gather_tick(0, 3)
+    gather_tick(1, 1)
+    expert(0, 0, 1)
+    expert(0, 0, 2)
     gather_tick(0, 4)
     gather_tick(1, 2)
+    expert(0, 0, 3)
+    expert(0, 1, 0)
     gather_tick(1, 3)
-    expert(0, 1)
+    expert(0, 1, 1)
+    expert(0, 1, 2)
+    expert(0, 1, 3)
     reduce_tick(0, (0, 1), *args)
     gather_tick(1, 4)
+    expert(1, 1, 0)
+    expert(1, 1, 1)
+    expert(1, 1, 2)
     reduce_tick(1, (0, 1), *args)
-    expert(1, 1)
+    expert(1, 1, 3)
     reduce_tick(0, (2, 3), *args)
+    expert(1, 0, 0)
     reduce_tick(2, (0, 1), *args)
-    expert(1, 0)
+    expert(1, 0, 1)
+    expert(1, 0, 2)
+    reduce_tick(3, (0, 1), *args)
+    expert(1, 0, 3)
     reduce_tick(1, (2, 3), *args)
-    reduce_tick(3, (0, 1), *args)
     combine(1)
     reduce_tick(0, (0, 1), *args2)
+    send_back(0)
     reduce_tick(2, (2, 3), *args)
-    send_back(0)
+    combine(0)
     reduce_tick(1, (0, 1), *args2)
-    combine(0)
     reduce_tick(3, (2, 3), *args)
     reduce_tick(2, (0, 1), *args2)
     send_back(1)
@@ -449,8 +457,7 @@
     for c in range(2):
         cols = pl.ds(1024 + 512 * c, 512)
         out_ref[:, cols] = (hid[:, cols].astype(F32) + reduce_last(c, *args2)).astype(BF16)
-    for d in range(1, 16):
-        back[d].wait_recv()
+    received(ret.at[pl.ds(1, 15)], ret_r)
     weight = [
         jnp.where(one[0], line[i : i + 1, :], 0.0) + jnp.where(one[1], line[i + 1 : i + 2, :], 0.0) for i in (2, 4)
     ]
@@ -466,8 +473,21 @@
         out_ref[:, cols] = (hid[:, cols].astype(F32) + acc).astype(BF16)
     cols = pl.ds(768, 256)
     out_ref[:, cols] = (hid[:, cols].astype(F32) + last).astype(BF16)
-    for c in pending:
+    sent(h_in, 0)
+    sent(h_docs, 1)
+    for c in g_duo + [w_duo] + e_duo:
         c.wait_send()
+    sent(meta.at[pl.ds(1, 7)], 4)
+    sent(part1.at[:, pl.ds(1, 7)], 6)
+    sent(tok.at[:, pl.ds(1, 7)], 10)
+    sent(outg.at[pl.ds(1, 15)], 11)
+    sent(out2.at[0, pl.ds(1, 15)], 12)
+    sent(out2.at[1, pl.ds(1, 15)], 13)
+    sent(xbuf.at[pl.ds(1, 7)], 14)
+    sent(y2.at[:, pl.ds(1, 15)], 15)
+    sent(part.at[pl.ds(1, 7)], 16)
+    sent(fin.at[pl.ds(1, 15)], 17)
+    sent(cpart.at[:, pl.ds(1, 7)], 18)
 
 
 def shards(
@@ -483,7 +503,7 @@
     scratch = [
         buf(512, 128), buf(512, 128), buf(512, 128), buf(3, 128), buf(4, 128, dtype=jnp.int32), buf(32, 2048),
         buf(16, 128), buf(2, 32, dtype=jnp.int32), buf(2, 32, dtype=F32),
-        buf(16, 128), buf(16, 128), buf(4, 128, dtype=jnp.int32), buf(528, 128, dtype=F32), buf(528, 128, dtype=F32),
+        buf(2, 16, 128), buf(4, 128, dtype=jnp.int32), buf(528, 128, dtype=F32), buf(528, 128, dtype=F32),
         buf(3, 256, 128), buf(256, 256), buf(2, 128, 2048), buf(4, 8, 32, 512), buf(4, 2, 4, 32, 512),
         buf(32, 2048), buf(32, 2048),
         buf(8, 32, dtype=F32), buf(8, 8, 128, dtype=F32), buf(128, 32), buf(3, 128, 32), buf(2, 384, 128),
@@ -492,10 +512,7 @@
         buf(256, 768), buf(192, 2048), buf(2, 192, 256), buf(2, 2048, 256), buf(2, 2048, 256), buf(2, 256, 2048),
         buf(8, 16, 8, 768), buf(4, 2, 4, 4, 8, 768), buf(2, 16, 24, 1024), buf(2, 16, 24, 1024), buf(2, 8, 32, 512),
         buf(2, 2, 4, 32, 512), buf(16, 8, 768), buf(16, 8, 768),
-        dma((13,)), dma((3,)), dma((3,)), dma((5,)), dma((5,)), dma((8,)), dma((8,)), dma((4, 2, 4)), dma((4, 2, 4)),
-        dma((2, 8)), dma((2, 8)), dma((16,)), dma((16,)), dma((4, 8)), dma((4, 8)),
-        dma((2, 16)), dma((2, 16)), dma((4, 2, 4)), dma((4, 2, 4)), dma((2, 16)), dma((2, 16)), dma((2, 2, 4)),
-        dma((2, 2, 4)), dma((16,)), dma((16,)),
+        dma((13,)), dma((19,)), dma((16,)), dma((7,)), dma((4, 7)), dma((4, 7)), dma((2, 7)), dma,
     ]
     return pl.pallas_call(
         kernel,

time: 97 us -> 91.6 us (0.944)
  Pallas kernels: 94.6 us -> 89.9 us
    pallas_call x1, Pallas kernels: 94.6 us -> 89.9 us  [shards(): pl.pallas_call(kernel, out_shape=jax.ShapeDtypeStruct((32, 2048), BF16),...]
where the time goes in v3:
time: 91.6 us; the launch traced here: 91.5 us
  Pallas kernels  89.9 us (98%)
  local copies, waits for them, and re-layouts  1.57 us (2%)
    pallas_call x1, Pallas kernels, shards(): pl.pallas_call(kernel, out_shape=jax.ShapeDtypeStruct((32, 2048), BF16),...  89.9 us

profile of v3, /device:TPU:2, one launch (start us, length us, event | category | flops | bytes accessed | tf_op | source)
XLA Modules:
  0.0 91.5 jit_solution(15465683053743619146)
XLA Ops:
  0.0 89.9 %layer.1 = bf16[32,2048]{1,0:T(8,128)(2,1)} custom-call(bf16[512,128]{1,0:T(8,128)(2,1)} %og_hbm.1, bf16[512,128]{1,0:T(8,128)(2,1)} %ig_hbm.1, bf16[512,128]{1,0:T(8,128)(2,1)} %ci_hbm.1, bf16[3,128]{1,0:T(4,128)(2,1)} %taps_hbm.1, s32[4,128]{1,0:T(4,128)} %bitcast.5, bf16[128,2048]{1,0:T(8,128)(2,1)} %ow_ref.1, bf16[32,2048]{1,0:T(8,128)(2,1)} %res_hbm.1, ...), custom_call_target="tpu_custom_call" | custom-call | tf_op jit(solution)/shard_map/layer/pallas_call | solution.py:517
  90.0 1.6 %copy.15 = bf16[32,2048]{1,0:T(8,128)(2,1)} copy(bf16[32,2048]{1,0:T(8,128)(2,1)} %layer.1) | data formatting | bytes 262144

commit v4 on v3

--- a/solution.py
+++ b/solution.py
@@ -199,9 +199,8 @@
     def reduce_tick(t, pieces, *rest):
         for piece in pieces:
             for way in range(2):
-                hop = t - (4 - len(REDUCE[piece % 2][way]))
-                if hop >= 0:
-                    reduce_hop(piece, way, hop, *rest)
+                if t < len(REDUCE[piece % 2][way]):
+                    reduce_hop(piece, way, t, *rest)
 
     def reduce_last(piece, part_at, rbuf_at, ssem, rsem):
         total = part_at(piece, 0)[...].astype(F32)
@@ -356,11 +355,6 @@
             for c in range(2):
                 y2[g, these, :, pl.ds(512 * c, 512)] = down(pl.ds(1024 + 512 * c, 512)).reshape(8, 24, 512)
 
-            for d in ORDER:
-                if d // 8 == pair:
-                    send(y2.at[g, d], back2.at[g, d], out_sem.at[15], in_sem.at[14 + g], behind(d))
-            if pair == 0:
-                back2[g, 0] = y2[g, 0]
         if step == 3:
             last = down(pl.ds(768, 256))
             for j in range(3):
@@ -368,6 +362,13 @@
                 packed = (dot(gmt[...], down(cols)) + dot(gtt[j], last)).astype(BF16)
                 for i, slot in enumerate(GROUPS[g]):
                     part[slot, these, :, cols] = packed[64 * i : 64 * i + 64].reshape(8, 8, 256)
+
+    def returns(pair, g):
+        for d in ORDER:
+            if d // 8 == pair:
+                send(y2.at[g, d], back2.at[g, d], out_sem.at[15], in_sem.at[14 + g], behind(d))
+        if pair == 0:
+            back2[g, 0] = y2[g, 0]
 
     args = (
         lambda p, s: piece_at(part, s, p),
@@ -405,10 +406,10 @@
     gather_tick(0, 0)
     tok_tick(2)
     disp2(0)
+    gather_tick(1, 0)
     gather_tick(0, 1)
     tok_tick(3)
     gather_tick(0, 2)
-    gather_tick(1, 0)
     tok_tick(4)
     disp2(1)
     for c in local[10:]:
@@ -420,33 +421,37 @@
     gather_tick(1, 1)
     expert(0, 0, 1)
     expert(0, 0, 2)
+    expert(0, 0, 3)
     gather_tick(0, 4)
     gather_tick(1, 2)
-    expert(0, 0, 3)
     expert(0, 1, 0)
-    gather_tick(1, 3)
     expert(0, 1, 1)
     expert(0, 1, 2)
+    returns(0, 1)
     expert(0, 1, 3)
     reduce_tick(0, (0, 1), *args)
+    expert(1, 0, 0)
+    gather_tick(1, 3)
+    returns(0, 0)
+    expert(1, 0, 1)
+    expert(1, 0, 2)
+    expert(1, 0, 3)
     gather_tick(1, 4)
+    reduce_tick(1, (0, 1), *args)
     expert(1, 1, 0)
     expert(1, 1, 1)
     expert(1, 1, 2)
-    reduce_tick(1, (0, 1), *args)
+    returns(1, 1)
+    returns(1, 0)
     expert(1, 1, 3)
     reduce_tick(0, (2, 3), *args)
-    expert(1, 0, 0)
     reduce_tick(2, (0, 1), *args)
-    expert(1, 0, 1)
-    expert(1, 0, 2)
+    reduce_tick(1, (2, 3), *args)
     reduce_tick(3, (0, 1), *args)
-    expert(1, 0, 3)
-    reduce_tick(1, (2, 3), *args)
     combine(1)
     reduce_tick(0, (0, 1), *args2)
+    reduce_tick(2, (2, 3), *args)
     send_back(0)
-    reduce_tick(2, (2, 3), *args)
     combine(0)
     reduce_tick(1, (0, 1), *args2)
     reduce_tick(3, (2, 3), *args)
@@ -454,9 +459,6 @@
     send_back(1)
     reduce_tick(3, (0, 1), *args2)
 
-    for c in range(2):
-        cols = pl.ds(1024 + 512 * c, 512)
-        out_ref[:, cols] = (hid[:, cols].astype(F32) + reduce_last(c, *args2)).astype(BF16)
     received(ret.at[pl.ds(1, 15)], ret_r)
     weight = [
         jnp.where(one[0], line[i : i + 1, :], 0.0) + jnp.where(one[1], line[i + 1 : i + 2, :], 0.0) for i in (2, 4)
@@ -473,6 +475,9 @@
         out_ref[:, cols] = (hid[:, cols].astype(F32) + acc).astype(BF16)
     cols = pl.ds(768, 256)
     out_ref[:, cols] = (hid[:, cols].astype(F32) + last).astype(BF16)
+    for c in range(2):
+        cols = pl.ds(1024 + 512 * c, 512)
+        out_ref[:, cols] = (hid[:, cols].astype(F32) + reduce_last(c, *args2)).astype(BF16)
     sent(h_in, 0)
     sent(h_docs, 1)
     for c in g_duo + [w_duo] + e_duo:

time: 91.6 us -> 87.5 us (0.955)
  Pallas kernels: 89.9 us -> 85.8 us
    pallas_call x1, Pallas kernels: 89.9 us -> 85.8 us  [shards(): pl.pallas_call(kernel, out_shape=jax.ShapeDtypeStruct((32, 2048), BF16),...]
where the time goes in v4:
time: 87.5 us; the launch traced here: 87.4 us
  Pallas kernels  85.8 us (98%)
  local copies, waits for them, and re-layouts  1.57 us (2%)
    pallas_call x1, Pallas kernels, shards(): pl.pallas_call(kernel, out_shape=jax.ShapeDtypeStruct((32, 2048), BF16),...  85.8 us

profile of v4, /device:TPU:2, one launch (start us, length us, event | category | flops | bytes accessed | tf_op | source)
XLA Modules:
  0.0 87.4 jit_solution(5927220932876315244)
XLA Ops:
  0.0 85.8 %layer.1 = bf16[32,2048]{1,0:T(8,128)(2,1)} custom-call(bf16[512,128]{1,0:T(8,128)(2,1)} %og_hbm.1, bf16[512,128]{1,0:T(8,128)(2,1)} %ig_hbm.1, bf16[512,128]{1,0:T(8,128)(2,1)} %ci_hbm.1, bf16[3,128]{1,0:T(4,128)(2,1)} %taps_hbm.1, s32[4,128]{1,0:T(4,128)} %bitcast.5, bf16[128,2048]{1,0:T(8,128)(2,1)} %ow_ref.1, bf16[32,2048]{1,0:T(8,128)(2,1)} %res_hbm.1, ...), custom_call_target="tpu_custom_call" | custom-call | tf_op jit(solution)/shard_map/layer/pallas_call | solution.py:522
  85.8 1.6 %copy.15 = bf16[32,2048]{1,0:T(8,128)(2,1)} copy(bf16[32,2048]{1,0:T(8,128)(2,1)} %layer.1) | data formatting | bytes 262144

commit v5 on v4

--- a/solution.py
+++ b/solution.py
@@ -38,12 +38,12 @@
 
 def kernel(
     og_hbm, ig_hbm, ci_hbm, taps_hbm, docs_hbm, ow_ref, res_hbm, gain_hbm, ids_hbm, rw_hbm, gw_ref, uw_ref, dw_ref,
-    out_ref,
+    hid, out_ref,
     og_ref, ig_ref, ci_ref, taps_ref, docs_ref, res_ref, gain_ref, ids_ref, rw_ref,
-    h_in, h_docs, ext, extd, gbuf, xa, wa, part1, rbuf1, hid, nrm,
+    h_in, h_docs, ext, extd, gbuf, xa, wa, part1, rbuf1, nrm,
     line, meta, tmain, ttail, tdisp, tcomb, gm, gt, gmt, gtt,
     tok, outg, out2, xbuf, x2buf, xcat, x2, act, wg, wu, wd, part, rbuf, y2, back2, cpart, rbuf2, fin, ret,
-    loc_sem, out_sem, in_sem, meta_r, ag_r, rs_r, tok_r, ret_r,
+    loc_sem, out_sem, in_sem, meta_r, ag_r, rs_r, tok_r, ret_r, pace_sem,
 ):
     sp = lax.axis_index("sp")
     tp = lax.axis_index("tp")
@@ -83,6 +83,15 @@
         pl.semaphore_signal(barrier, inc=1, device_id=device, device_id_type=MESH)
     for d in range(1, 16):
         pl.semaphore_signal(barrier, inc=1, device_id=ahead(d), device_id_type=MESH)
+
+    def pace():
+        @pl.when(core == 0)
+        def _():
+            pl.semaphore_signal(pace_sem, inc=1, device_id=partner, device_id_type=MESH)
+
+        @pl.when(core == 1)
+        def _():
+            pl.semaphore_wait(pace_sem, 1)
 
     pairs = [
         (ids_hbm, ids_ref), (rw_hbm, rw_ref), (ig_hbm, ig_ref), (ci_hbm, ci_ref), (docs_hbm, docs_ref),
@@ -137,7 +146,15 @@
     send(ci_ref.at[pl.ds(496, 16)], h_in.at[1], out_sem.at[0], in_sem.at[0], following)
     send(docs_ref, h_docs, out_sem.at[1], in_sem.at[1], following)
     rest = pl.ds(32, 224)
-    g_duo = [send(gbuf.at[1 - core, rest], gbuf.at[2, rest], out_sem.at[2], in_sem.at[2], partner)]
+    g_duo = send(gbuf.at[1 - core, rest], gbuf.at[2, rest], out_sem.at[2], in_sem.at[2], partner)
+    head = pl.ds(0, 32)
+
+    def first_block(where):
+        @pl.when(core == 1 - where)
+        def _():
+            send(gbuf.at[where, head], gbuf.at[2, head], out_sem.at[5], in_sem.at[4], partner)
+
+    first_block(1)
     local[7].wait()
     w_duo = send(wa.at[0], wa.at[1], out_sem.at[3], in_sem.at[3], partner)
 
@@ -157,17 +174,6 @@
                 send(meta.at[slots[k]], meta.at[to], out_sem.at[4], meta_r.at[to - 1], sides[way])
 
     meta_tick(0)
-    received(h_in, in_sem.at[0])
-    received(h_docs, in_sem.at[1])
-    ext[pl.ds(0, 16), :] = h_in[0].astype(F32) * h_in[1].astype(F32)
-    old = jnp.broadcast_to(h_docs[...].astype(F32)[3:4, :], (128, 128)).T
-    extd[pl.ds(0, 16), :] = old[112:128, :]
-    gbuf[0, pl.ds(0, 32), :] = gated(0, 32)
-    rest = pl.ds(0, 32)
-    g_duo.append(send(gbuf.at[1 - core, rest], gbuf.at[2, rest], out_sem.at[5], in_sem.at[4], partner))
-    e_duo.append(send(dw_ref.at[0], wd.at[1], out_sem.at[9], in_sem.at[7], partner))
-    xa[:, pl.ds(0, 128)] = gbuf[core]
-
     rows = iota((128, 32), 0)
     rel, sub = rows >> 3, (rows & 7).astype(F32)
     one = [(jnp.broadcast_to(rid[k : k + 1, :], (128, 32)) == rel) for k in range(2)]
@@ -179,11 +185,6 @@
         hit = ((sub == 6.0) & (place == float(j))) | ((sub == 7.0) & (place == j + 3.0))
         ttail[j] = (jnp.where(hit, 1.0, 0.0) * both).astype(BF16)
 
-    w_duo.wait_recv()
-    for c in g_duo:
-        c.wait_recv()
-    xa[:, pl.ds(128, 128)] = gbuf[2]
-
     def arrival(rsem, piece, way, hop):
         return rsem.at[piece, hop if way == 0 else len(REDUCE[piece % 2][0]) + hop]
 
@@ -217,11 +218,41 @@
         out_sem.at[6],
         rs_r,
     )
+    def first_hop(piece, late):
+        for way in range(2):
+            slot = REDUCE[piece % 2][way][0]
+            ready = lax.rem(z - slot + 8, 8) == 0
+
+            @pl.when(ready if late else jnp.logical_not(ready))
+            def _():
+                reduce_hop(piece, way, 0, *args1)
+
+    xa[rest, pl.ds(0, 128)] = gbuf[core, rest]
+    w_duo.wait_recv()
+    g_duo.wait_recv()
+    xa[rest, pl.ds(128, 128)] = gbuf[2, rest]
     for p in range(4):
         cols = pl.ds(512 * p, 512)
-        prod = dot(xa[:, pl.ds(0, 128)], wa[0, :, cols]) + dot(xa[:, pl.ds(128, 128)], wa[1, :, cols])
-        part1[p] = prod.astype(BF16).reshape(8, 32, 512)
-        reduce_tick(0, (p,), *args1)
+        prod = dot(xa[rest, pl.ds(0, 128)], wa[0, :, cols]) + dot(xa[rest, pl.ds(128, 128)], wa[1, :, cols])
+        part1[p, pl.ds(1, 7)] = prod.astype(BF16).reshape(7, 32, 512)
+        first_hop(p, False)
+    received(h_in, in_sem.at[0])
+    received(h_docs, in_sem.at[1])
+    ext[pl.ds(0, 16), :] = h_in[0].astype(F32) * h_in[1].astype(F32)
+    old = jnp.broadcast_to(h_docs[...].astype(F32)[3:4, :], (128, 128)).T
+    extd[pl.ds(0, 16), :] = old[112:128, :]
+    gbuf[0, head, :] = gated(0, 32)
+    first_block(0)
+    e_duo.append(send(dw_ref.at[0], wd.at[1], out_sem.at[9], in_sem.at[7], partner))
+    xa[head, pl.ds(0, 128)] = gbuf[core, head]
+    received(gbuf.at[2, head], in_sem.at[4])
+    xa[head, pl.ds(128, 128)] = gbuf[2, head]
+    for p in range(4):
+        cols = pl.ds(512 * p, 512)
+        prod = dot(xa[head, pl.ds(0, 128)], wa[0, :, cols]) + dot(xa[head, pl.ds(128, 128)], wa[1, :, cols])
+        part1[p, 0] = prod.astype(BF16)
+        first_hop(p, True)
+
     def selections(axis, main, tails):
         shape = (192, 256) if axis == 0 else (256, 192)
         d, k, r = natural(iota(shape, axis))
@@ -258,6 +289,7 @@
     reduce_tick(1, range(4), *args1)
     meta_tick(2)
     tables(0)
+    pace()
     reduce_tick(2, range(4), *args1)
     meta_tick(3)
     selections(1, gmt, gtt)
@@ -472,16 +504,17 @@
         for w in weight:
             acc = acc + dot_t(w * tmain[...], block)
             last = last + dot_t(w * ttail[j], block)
-        out_ref[:, cols] = (hid[:, cols].astype(F32) + acc).astype(BF16)
+        out_ref[:, cols] = acc
     cols = pl.ds(768, 256)
-    out_ref[:, cols] = (hid[:, cols].astype(F32) + last).astype(BF16)
+    out_ref[:, cols] = last
     for c in range(2):
         cols = pl.ds(1024 + 512 * c, 512)
-        out_ref[:, cols] = (hid[:, cols].astype(F32) + reduce_last(c, *args2)).astype(BF16)
+        out_ref[:, cols] = reduce_last(c, *args2)
     sent(h_in, 0)
     sent(h_docs, 1)
-    for c in g_duo + [w_duo] + e_duo:
+    for c in [g_duo, w_duo] + e_duo:
         c.wait_send()
+    sent(gbuf.at[2, pl.ds(0, 32)], 5)
     sent(meta.at[pl.ds(1, 7)], 4)
     sent(part1.at[:, pl.ds(1, 7)], 6)
     sent(tok.at[:, pl.ds(1, 7)], 10)
@@ -510,20 +543,20 @@
         buf(16, 128), buf(2, 32, dtype=jnp.int32), buf(2, 32, dtype=F32),
         buf(2, 16, 128), buf(4, 128, dtype=jnp.int32), buf(528, 128, dtype=F32), buf(528, 128, dtype=F32),
         buf(3, 256, 128), buf(256, 256), buf(2, 128, 2048), buf(4, 8, 32, 512), buf(4, 2, 4, 32, 512),
-        buf(32, 2048), buf(32, 2048),
+        buf(32, 2048),
         buf(8, 32, dtype=F32), buf(8, 8, 128, dtype=F32), buf(128, 32), buf(3, 128, 32), buf(2, 384, 128),
         buf(2, 2, 384, 128), buf(192, 256), buf(3, 192, 256), buf(256, 192), buf(3, 256, 192),
         buf(2, 8, 32, 512), buf(16, 8, 768), buf(2, 16, 24, 1024), buf(8, 16, 8, 768), buf(2, 16, 24, 1024),
         buf(256, 768), buf(192, 2048), buf(2, 192, 256), buf(2, 2048, 256), buf(2, 2048, 256), buf(2, 256, 2048),
         buf(8, 16, 8, 768), buf(4, 2, 4, 4, 8, 768), buf(2, 16, 24, 1024), buf(2, 16, 24, 1024), buf(2, 8, 32, 512),
         buf(2, 2, 4, 32, 512), buf(16, 8, 768), buf(16, 8, 768),
-        dma((13,)), dma((19,)), dma((16,)), dma((7,)), dma((4, 7)), dma((4, 7)), dma((2, 7)), dma,
+        dma((13,)), dma((19,)), dma((16,)), dma((7,)), dma((4, 7)), dma((4, 7)), dma((2, 7)), dma, pltpu.SemaphoreType.REGULAR,
     ]
-    return pl.pallas_call(
+    hid, total = pl.pallas_call(
         kernel,
-        out_shape=jax.ShapeDtypeStruct((32, 2048), BF16),
+        out_shape=(pltpu.VMEM((32, 2048), BF16), pltpu.VMEM((32, 2048), F32)),
         in_specs=[hbm] * 13,
-        out_specs=pl.BlockSpec(memory_space=pltpu.VMEM),
+        out_specs=(pl.BlockSpec(memory_space=pltpu.VMEM),) * 2,
         scratch_shapes=scratch,
         compiler_params=pltpu.CompilerParams(
             collective_id=0, has_side_effects=True, vmem_limit_bytes=56 * 1024 * 1024
@@ -533,6 +566,7 @@
         out_gate, in_gate, conv_input, conv_taps, documents.reshape(4, 128), out_weight, residual,
         norm_gain.reshape(16, 128), expert_ids.T, route_weights.T, gate_weight, up_weight, down_weight,
     )
+    return (hid.astype(F32) + total).astype(BF16)
 
 
 def solution(mesh):

time: 87.5 us -> 85.3 us (0.975); the launches traced: 87.4 us -> 84.3 us
  Pallas kernels: 85.8 us -> 83.6 us
  local copies, waits for them, and re-layouts: 1.57 us -> 0 us
    pallas_call x1, Pallas kernels: 85.8 us -> 83.6 us  [shards(): pl.pallas_call(kernel, out_shape=(pltpu.VMEM((32, 2048), BF16), pltpu.VME...]
    unnamed x1 -> x0, local copies, waits for them, and re-layouts: 1.57 us -> none
where the time goes in v5:
time: 85.3 us; the launch traced here: 84.3 us
  Pallas kernels  83.6 us (98%)
    pallas_call x1, Pallas kernels, shards(): pl.pallas_call(kernel, out_shape=(pltpu.VMEM((32, 2048), BF16), pltpu.VME...  83.6 us

profile of v5, /device:TPU:2, one launch (start us, length us, event | category | flops | bytes accessed | tf_op | source)
XLA Modules:
  0.0 84.3 jit_solution(6634229492850874128)
XLA Ops:
  0.0 83.6 %layer.1 = (bf16[32,2048]{1,0:T(8,128)(2,1)S(1)}, f32[32,2048]{1,0:T(8,128)S(1)}) custom-call(bf16[512,128]{1,0:T(8,128)(2,1)} %og_hbm.1, bf16[512,128]{1,0:T(8,128)(2,1)} %ig_hbm.1, bf16[512,128]{1,0:T(8,128)(2,1)} %ci_hbm.1, bf16[3,128]{1,0:T(4,128)(2,1)} %taps_hbm.1, s32[4,128]{1,0:T(4,128)} %bitcast.5, bf16[128,2048]{1,0:T(8,128)(2,1)} %ow_ref.1, ...), custom_call_target="tpu_custom_call" | custom-call | tf_op jit(solution)/shard_map/layer/pallas_call | solution.py:555
  83.6 0.7 add_convert_fusion

commit v6 on v5

--- a/solution.py
+++ b/solution.py
@@ -468,8 +468,8 @@
     expert(1, 0, 1)
     expert(1, 0, 2)
     expert(1, 0, 3)
+    reduce_tick(1, (0, 1), *args)
     gather_tick(1, 4)
-    reduce_tick(1, (0, 1), *args)
     expert(1, 1, 0)
     expert(1, 1, 1)
     expert(1, 1, 2)

time: 85.3 us -> 84 us (0.985)
  no operation moved by 1% of the time
where the time goes in v6:
time: 84 us; the launch traced here: 83.6 us
  Pallas kernels  82.9 us (99%)
    pallas_call x1, Pallas kernels, shards(): pl.pallas_call(kernel, out_shape=(pltpu.VMEM((32, 2048), BF16), pltpu.VME...  82.9 us

profile of v6, /device:TPU:2, one launch (start us, length us, event | category | flops | bytes accessed | tf_op | source)
XLA Modules:
  0.0 83.6 jit_solution(13573755757306448037)
XLA Ops:
  0.0 82.9 %layer.1 = (bf16[32,2048]{1,0:T(8,128)(2,1)S(1)}, f32[32,2048]{1,0:T(8,128)S(1)}) custom-call(bf16[512,128]{1,0:T(8,128)(2,1)} %og_hbm.1, bf16[512,128]{1,0:T(8,128)(2,1)} %ig_hbm.1, bf16[512,128]{1,0:T(8,128)(2,1)} %ci_hbm.1, bf16[3,128]{1,0:T(4,128)(2,1)} %taps_hbm.1, s32[4,128]{1,0:T(4,128)} %bitcast.5, bf16[128,2048]{1,0:T(8,128)(2,1)} %ow_ref.1, ...), custom_call_target="tpu_custom_call" | custom-call | tf_op jit(solution)/shard_map/layer/pallas_call | solution.py:555
  82.9 0.7 add_convert_fusion
